TPU v7x, 32 devices: a whole 2x2x4 slice. The times are simulated.
32 devices in a mesh: sp: 8 (over z, x), tp: 4 (over y, core).
Axes of the slice: x: 2, y: 2, z: 4, core: 2. Of those that a mesh axis runs over, the one named last changes fastest.
Arguments:
- query_one: bfloat16 [2048, 512], P('sp', 'tp'), may hold values from -100 to 100, as said below
- key_one: bfloat16 [2048, 512], P('sp', 'tp'), may hold values from -8 to 8
- query_two: bfloat16 [2048, 512], P('sp', 'tp'), may hold values from -100 to 100, as said below
- key_two: bfloat16 [2048, 512], P('sp', 'tp'), may hold values from -8 to 8
- values: bfloat16 [2048, 1024], P('sp', 'tp'), may hold values from -6 to 6
- mix_lambda: float32 [8], P('tp'), may hold values from 0.3 to 0.8
- head_gain: float32 [128], replicated, may hold values from 0.1 to 1.9
- residual_in: bfloat16 [2048, 2048], P(('sp', 'tp')), may hold values from -6 to 6
- out_weight: bfloat16 [1024, 2048], replicated, may hold values from -0.1875 to 0.1875
- norm_gain: float32 [2048], replicated, may hold values from 0.1 to 1.9
- route_ids: int32 [2048, 2], P(('sp', 'tp')), may hold values from 0 to 15, all different within a row; in each aligned block of 64 rows (0 to 63, 64 to 127, ...) at most 16 rows name the same one
- route_logits: float32 [2048, 2], P(('sp', 'tp')), may hold values from -6 to 6
- group_prob: float32 [2048], P(('sp', 'tp')), may hold values from 0.25 to 1
- gate_weight: bfloat16 [16, 2048, 1024], P('sp', None, 'tp'), may hold values from -0.125 to 0.125
- up_weight: bfloat16 [16, 2048, 1024], P('sp', None, 'tp'), may hold values from -0.125 to 0.125
- down_weight: bfloat16 [16, 1024, 2048], P('sp', 'tp'), may hold values from -0.1875 to 0.1875
Outputs:
- layer_out: bfloat16 [2048, 2048], P(('sp', 'tp'))
Inputs may be any that keep to these rules, and one draw needn't show every extreme that they name: `query_one`: drawn together with key_one. `query_two`: drawn together with key_two. `route_ids`: the experts of a row differ. In the rows of one device no expert is named more than 16 times, a bound that some block reaches.
All inputs are finite; a program needn't handle non-finite values.
Results may differ from a plain program's by a relative error of at most 0.014.
Values may be sent and summed in bfloat16 or wider, within the bound.
A program may use at most 128 MiB of HBM per device.

v0:
```python
import functools
import math

import jax
import jax.numpy as jnp
from jax import lax
from jax.experimental import pallas as pl
from jax.experimental.pallas import tpu as pltpu
from jax.sharding import PartitionSpec as P

norm_epsilon = 1e-06
MESH = pl.DeviceIdType.MESH
VMEM_LIMIT = 60 * 1024 * 1024


def pair_of(count):
    return 2 if count % 2 == 0 else 1


def greet(peers):
    barrier = pltpu.get_barrier_semaphore()
    for peer in peers:
        pl.semaphore_signal(barrier, inc=1, device_id=peer, device_id_type=MESH)
    pl.semaphore_wait(barrier, len(peers))


def attend_kernel(
    n_sp,
    n_tp,
    vd,
    k1_ref,
    k2_ref,
    v_ref,
    q1_ref,
    q2_ref,
    lam_ref,
    gain_ref,
    out_ref,
    kvp,
    qp,
    held,
    q_far,
    m_ref,
    l_ref,
    acc_ref,
    stage,
    cross_send,
    cross_recv,
    line_send,
    line_recv,
    side_send,
    side_recv,
    head_send,
    head_recv,
):
    inner = pair_of(n_sp)
    length = n_sp // inner
    half = length // 2
    me = lax.axis_index("sp")
    mt = lax.axis_index("tp")
    z, x = me // inner, me % inner
    head, zi = z // half, z % half
    rows = q1_ref.shape[0]
    qk = q1_ref.shape[1] // 2
    scale = 1.0 / math.sqrt(qk)
    exact = math.frexp(scale)[0] == 0.5
    early, after = (scale, 1.0) if exact else (1.0, scale)
    other = z * inner + (inner - 1 - x)
    mirror = (length - 1 - z) * inner + x
    far_zi = half - 1 - zi
    for h in range(2):
        kvp[h, :, 0:qk] = k1_ref[:, h * qk : (h + 1) * qk]
        kvp[h, :, qk : 2 * qk] = k2_ref[:, h * qk : (h + 1) * qk]
        kvp[h, :, 2 * qk : 2 * qk + vd] = v_ref[:, h * vd : (h + 1) * vd]
        qp[h, :, 0:qk] = q1_ref[:, h * qk : (h + 1) * qk] * jnp.bfloat16(early)
        qp[h, :, qk : 2 * qk] = q2_ref[:, h * qk : (h + 1) * qk] * jnp.bfloat16(early)

    def line_device(zz):
        return (head * half + zz) * inner + x

    peers = [{"sp": me, "tp": (mt + t) % n_tp} for t in range(1, n_tp)]
    peers += [{"sp": mirror, "tp": (mt + t) % n_tp} for t in range(n_tp)]
    if inner == 2:
        peers.append({"sp": other, "tp": mt})
    if half > 1:
        for shift in sorted({1, half - 1}):
            peers.append({"sp": line_device((zi + shift) % half), "tp": mt})
    greet(peers)

    def remote(src, dst, send, recv, sp):
        return pltpu.make_async_remote_copy(
            src_ref=src,
            dst_ref=dst,
            send_sem=send,
            recv_sem=recv,
            device_id={"sp": sp, "tp": mt},
            device_id_type=MESH,
        )

    cross_q = remote(qp.at[1 - head], q_far, cross_send.at[0], cross_recv.at[0], mirror)
    cross_kv = remote(
        kvp.at[1 - head], held.at[1, far_zi, x], cross_send.at[1], cross_recv.at[1], mirror
    )

    def line_copy(j, src, zz, way):
        ahead = jnp.clip(jnp.where(way == 0, zi + 1, zi - 1), 0, half - 1)
        return remote(
            src,
            held.at[j, zz, x],
            line_send.at[j, way, zz],
            line_recv.at[j, zz],
            line_device(ahead),
        )

    def side_copy(j, src, zz):
        return remote(src, held.at[j, zz, x], side_send.at[j, zz], side_recv.at[j, zz], other)

    def start_from(j, src):
        @pl.when(zi + 1 < half)
        def _():
            line_copy(j, src, zi, 0).start()

        @pl.when(zi > 0)
        def _():
            line_copy(j, src, zi, 1).start()

        if inner == 2:
            side_copy(j, src, zi).start()

    own = kvp.at[head]
    cross_kv.start()
    start_from(0, own)
    cross_q.start()
    m_ref[...] = jnp.full(m_ref.shape, -1e30, jnp.float32)
    l_ref[...] = jnp.zeros(l_ref.shape, jnp.float32)
    acc_ref[...] = jnp.zeros(acc_ref.shape, jnp.float32)

    def absorb(block, q_ref, group):
        vals = block[:, 2 * qk : 2 * qk + vd]
        for which in range(2):
            at = 2 * group + which
            scores = lax.dot_general(
                q_ref[:, which * qk : (which + 1) * qk],
                block[:, which * qk : (which + 1) * qk],
                (((1,), (1,)), ((), ())),
                preferred_element_type=jnp.float32,
            )
            if after != 1.0:
                scores = scores * after
            old = m_ref[at]
            new = jnp.maximum(old, jnp.max(scores, axis=1, keepdims=True))
            shrink = jnp.exp(old - new)
            expo = jnp.exp(scores - new[:, :1])
            m_ref[at] = new
            l_ref[at] = l_ref[at] * shrink + jnp.sum(expo, axis=1, keepdims=True)
            acc_ref[at] = acc_ref[at] * shrink[:, :1] + jnp.dot(
                expo.astype(jnp.bfloat16), vals, preferred_element_type=jnp.float32
            )

    q_own = qp.at[head]

    def absorb_both(block):
        absorb(block, q_own, 0)
        absorb(block, q_far, 1)

    def place(n):
        dist = (n + 1) // 2
        return jnp.where(n % 2 == 1, zi - dist, zi + dist), 1 - n % 2

    def line_steps(j, take):
        def line_step(n, carry):
            zz, way = place(n)

            @pl.when((zz >= 0) & (zz < half))
            def _():
                block = held.at[j, zz, x]
                line_copy(j, block, zz, way).wait_recv()
                ahead = jnp.where(way == 0, zi + 1, zi - 1)

                @pl.when((ahead >= 0) & (ahead < half))
                def _():
                    line_copy(j, block, zz, way).start()

                if inner == 2:
                    side_copy(j, block, zz).start()
                take(block)

            return carry

        lax.fori_loop(1, 2 * half - 1, line_step, 0)

    def line_again(j):
        def again(n, carry):
            zz, _ = place(n)

            @pl.when((zz >= 0) & (zz < half))
            def _():
                absorb(held.at[j, zz, x], q_far, 1)

            return carry

        lax.fori_loop(1, 2 * half - 1, again, 0)

    def side_steps(j, begin):
        def side_step(n, carry):
            zz, _ = place(n)

            @pl.when((zz >= 0) & (zz < half))
            def _():
                block = held.at[j, zz, 1 - x]
                side_copy(j, block, zz).wait_recv()
                absorb_both(block)

            return carry

        lax.fori_loop(begin, 2 * half - 1, side_step, 0)

    near = held.at[0, zi, 1 - x]
    far = held.at[1, zi, x]
    absorb(own, q_own, 0)
    if inner == 2:
        side_copy(0, near, zi).wait_recv()
        absorb(near, q_own, 0)
    line_steps(0, lambda block: absorb(block, q_own, 0))
    cross_kv.wait_recv()
    start_from(1, far)
    absorb(far, q_own, 0)
    cross_q.wait_recv()
    absorb(own, q_far, 1)
    absorb(far, q_far, 1)
    line_steps(1, absorb_both)
    line_again(0)
    if inner == 2:
        absorb(near, q_far, 1)
        side_steps(0, 1)
        side_steps(1, 0)

    share = rows // n_tp
    lam = lam_ref[head]
    columns = pl.ds(pl.multiple_of((mt * 2 + head) * vd, vd), vd)
    copies = []
    for group, sp in ((1, mirror), (0, me)):
        read_a = acc_ref[2 * group] / l_ref[2 * group][:, :1]
        read_b = acc_ref[2 * group + 1] / l_ref[2 * group + 1][:, :1]
        combined = read_a - lam * read_b
        combined = (
            combined
            * lax.rsqrt(jnp.mean(combined * combined, axis=-1, keepdims=True) + norm_epsilon)
            * gain_ref[...]
        )
        stage[group] = combined.astype(jnp.bfloat16)
        for t in range(n_tp):
            to = (mt + t) % n_tp
            span = pl.ds(pl.multiple_of(to * share, share), share)
            if group == 0 and t == 0:
                out_ref[:, columns] = stage[0, span, :]
                continue
            copy = pltpu.make_async_remote_copy(
                src_ref=stage.at[group, span],
                dst_ref=out_ref.at[:, columns],
                send_sem=head_send.at[group, t],
                recv_sem=head_recv.at[group, t],
                device_id={"sp": sp, "tp": to},
                device_id_type=MESH,
            )
            copy.start()
            copies.append(copy)

    cross_q.wait_send()
    cross_kv.wait_send()
    for j in range(2):

        def drain(n, carry):
            zz, way = place(n)

            @pl.when((zz >= 0) & (zz < half))
            def _():
                ahead = jnp.where(way == 0, zi + 1, zi - 1)

                @pl.when((ahead >= 0) & (ahead < half))
                def _():
                    line_copy(j, own, zz, way).wait_send()

                if inner == 2:
                    side_copy(j, own, zz).wait_send()

            return carry

        lax.fori_loop(1, 2 * half - 1, drain, 0)

        @pl.when(zi + 1 < half)
        def _():
            line_copy(j, own, zi, 0).wait_send()

        @pl.when(zi > 0)
        def _():
            line_copy(j, own, zi, 1).wait_send()

        if inner == 2:
            side_copy(j, own, zi).wait_send()
    for copy in copies:
        copy.wait()


def attend(n_sp, n_tp, k1, k2, v, q1, q2, lam, gain):
    rows = q1.shape[0]
    inner = pair_of(n_sp)
    half = n_sp // inner // 2
    assert lam.shape[0] == 2 and half * inner * 2 == n_sp
    vd = v.shape[1] // 2
    qk = q1.shape[1] // 2
    cols = 2 * qk + vd
    vmem = pl.BlockSpec(memory_space=pltpu.VMEM)
    dma = pltpu.SemaphoreType.DMA
    return pl.pallas_call(
        functools.partial(attend_kernel, n_sp, n_tp, vd),
        out_shape=jax.ShapeDtypeStruct((rows // n_tp, n_tp * 2 * vd), jnp.bfloat16),
        in_specs=[vmem] * 5 + [pl.BlockSpec(memory_space=pltpu.SMEM), vmem],
        out_specs=vmem,
        scratch_shapes=[
            pltpu.VMEM((2, rows, cols), jnp.bfloat16),
            pltpu.VMEM((2, rows, 2 * qk), jnp.bfloat16),
            pltpu.VMEM((2, half, inner, rows, cols), jnp.bfloat16),
            pltpu.VMEM((rows, 2 * qk), jnp.bfloat16),
            pltpu.VMEM((4, rows, 128), jnp.float32),
            pltpu.VMEM((4, rows, 128), jnp.float32),
            pltpu.VMEM((4, rows, vd), jnp.float32),
            pltpu.VMEM((2, rows, vd), jnp.bfloat16),
            dma((2,)),
            dma((2,)),
            dma((2, 2, half)),
            dma((2, half)),
            dma((2, half)),
            dma((2, half)),
            dma((2, n_tp)),
            dma((2, n_tp)),
        ],
        compiler_params=pltpu.CompilerParams(
            collective_id=0, has_side_effects=True, vmem_limit_bytes=VMEM_LIMIT
        ),
    )(k1, k2, v, q1, q2, lam, gain)


def tp_peers(n_tp):
    inner = pair_of(n_tp)
    mt = lax.axis_index("tp")
    o, c = mt // inner, mt % inner
    across = [((o + d) % (n_tp // inner)) * inner + c for d in range(1, n_tp // inner)]
    return inner, across, o * inner + (inner - 1 - c)


def greet_all(n_sp, n_tp):
    me, mt = lax.axis_index("sp"), lax.axis_index("tp")
    inner, across, partner = tp_peers(n_tp)
    peers = [{"sp": (me + s) % n_sp, "tp": mt} for s in range(1, n_sp)]
    peers += [{"sp": me, "tp": t} for t in across]
    if inner == 2:
        peers.append({"sp": me, "tp": partner})
    greet(peers)


def dispatch_kernel(
    n_sp, n_tp, rows_ref, out_ref, sp_send, sp_recv, y_send, y_recv, c_send, c_recv, own_sem
):
    me, mt = lax.axis_index("sp"), lax.axis_index("tp")
    inner, across, partner = tp_peers(n_tp)
    groups = n_tp // inner
    o = mt // inner
    greet_all(n_sp, n_tp)

    def sp_copy(d):
        to = (me + d) % n_sp
        return pltpu.make_async_remote_copy(
            src_ref=rows_ref.at[to],
            dst_ref=out_ref.at[:, mt, me],
            send_sem=sp_send.at[d],
            recv_sem=sp_recv.at[d],
            device_id={"sp": to, "tp": mt},
            device_id_type=MESH,
        )

    def tp_copy(t, s, to, send, recv):
        return pltpu.make_async_remote_copy(
            src_ref=out_ref.at[:, t, s],
            dst_ref=out_ref.at[:, t, s],
            send_sem=send,
            recv_sem=recv,
            device_id={"sp": me, "tp": to},
            device_id_type=MESH,
        )

    order = sorted(range(1, n_sp), key=lambda d: min(d, n_sp - d))
    for d in reversed(order):
        sp_copy(d).start()
    own = pltpu.make_async_copy(rows_ref.at[me], out_ref.at[:, mt, me], own_sem)
    own.start()
    own.wait()
    started = []

    def spread(d):
        s = (me - d + n_sp) % n_sp
        for g in range(1, groups):
            copy = tp_copy(mt, s, across[g - 1], y_send.at[g, d], y_recv.at[g, d])
            copy.start()
            started.append(copy)
        if inner == 2:
            copy = tp_copy(mt, s, partner, c_send.at[0, d], c_recv.at[0, d])
            copy.start()
            started.append(copy)

    def relay(d):
        s = (me - d + n_sp) % n_sp
        for g in range(1, groups):
            source = ((o - g + groups) % groups) * inner + mt % inner
            tp_copy(source, s, partner, y_send.at[g, d], y_recv.at[g, d]).wait_recv()
            if inner == 2:
                copy = tp_copy(source, s, partner, c_send.at[g, d], c_recv.at[g, d])
                copy.start()
                started.append(copy)

    order = order[::-1]
    sequence = [0] + order
    spread(0)
    for i, d in enumerate(order):
        sp_copy(d).wait_recv()
        spread(d)
        relay(sequence[i])
    relay(sequence[-1])
    for d in range(n_sp):
        s = (me - d + n_sp) % n_sp
        if inner == 2:
            for g in range(groups):
                source = ((o - g + groups) % groups) * inner + (1 - mt % inner)
                tp_copy(source, s, partner, c_send.at[g, d], c_recv.at[g, d]).wait_recv()
    for copy in started:
        copy.wait_send()
    for d in order:
        sp_copy(d).wait_send()


def dispatch(n_sp, n_tp, rows):
    _, experts, cap, width = rows.shape
    groups = n_tp // pair_of(n_tp)
    sem = pltpu.SemaphoreType.DMA
    hbm = pl.BlockSpec(memory_space=pltpu.VMEM)
    return pl.pallas_call(
        functools.partial(dispatch_kernel, n_sp, n_tp),
        out_shape=jax.ShapeDtypeStruct((experts, n_tp, n_sp, cap, width), rows.dtype),
        in_specs=[hbm],
        out_specs=pl.BlockSpec(memory_space=pl.ANY),
        scratch_shapes=[
            sem((n_sp,)),
            sem((n_sp,)),
            sem((groups, n_sp)),
            sem((groups, n_sp)),
            sem((groups, n_sp)),
            sem((groups, n_sp)),
            sem,
        ],
        compiler_params=pltpu.CompilerParams(
            collective_id=1, has_side_effects=True, vmem_limit_bytes=VMEM_LIMIT
        ),
    )(rows)


def collect_kernel(
    n_sp,
    n_tp,
    part_ref,
    out_ref,
    from_core,
    from_across,
    summed,
    total,
    c_send,
    c_recv,
    y_send,
    y_recv,
    sp_send,
    sp_recv,
):
    me, mt = lax.axis_index("sp"), lax.axis_index("tp")
    inner, across, partner = tp_peers(n_tp)
    groups = n_tp // inner
    o, c = mt // inner, mt % inner
    greet_all(n_sp, n_tp)
    order = sorted(range(1, n_sp), key=lambda d: min(d, n_sp - d), reverse=True) + [0]

    def to_of(d):
        return (me + d) % n_sp

    def core_copy(d, g):
        row = ((o + g) % groups) * inner + (inner - 1 - c)
        return pltpu.make_async_remote_copy(
            src_ref=part_ref.at[:, row, to_of(d)],
            dst_ref=from_core.at[d, g],
            send_sem=c_send.at[d, g],
            recv_sem=c_recv.at[d, g],
            device_id={"sp": me, "tp": partner},
            device_id_type=MESH,
        )

    def across_copy(d, g):
        return pltpu.make_async_remote_copy(
            src_ref=summed.at[d, g],
            dst_ref=from_across.at[d, g],
            send_sem=y_send.at[d, g],
            recv_sem=y_recv.at[d, g],
            device_id={"sp": me, "tp": across[g - 1]},
            device_id_type=MESH,
        )

    def sp_copy(d):
        return pltpu.make_async_remote_copy(
            src_ref=total.at[d],
            dst_ref=out_ref.at[me],
            send_sem=sp_send.at[d],
            recv_sem=sp_recv.at[d],
            device_id={"sp": to_of(d), "tp": mt},
            device_id_type=MESH,
        )

    if inner == 2:
        for d in order:
            for g in list(range(1, groups)) + [0]:
                core_copy(d, g).start()

    def pair_sum(d, g):
        row = ((o + g) % groups) * inner + c
        value = part_ref[:, row, to_of(d)].astype(jnp.float32)
        if inner == 2:
            core_copy(d, g).wait_recv()
            value = value + from_core[d, g].astype(jnp.float32)
        return value

    def first(d):
        for g in range(1, groups):
            summed[d, g] = pair_sum(d, g).astype(summed.dtype)
            across_copy(d, g).start()

    def second(d):
        value = pair_sum(d, 0)
        for g in range(1, groups):
            across_copy(d, g).wait_recv()
            value = value + from_across[d, g].astype(jnp.float32)
        value = value.astype(total.dtype)
        if d == 0:
            out_ref[me] = value
        else:
            total[d] = value
            sp_copy(d).start()

    ahead = min(3, n_sp)
    for d in order[:ahead]:
        first(d)
    for i, d in enumerate(order):
        second(d)
        if i + ahead < n_sp:
            first(order[i + ahead])
    for d in range(1, n_sp):
        sp_copy(d).wait_recv()
    for d in range(n_sp):
        if d:
            sp_copy(d).wait_send()
        for g in range(groups):
            if g:
                across_copy(d, g).wait_send()
            if inner == 2:
                core_copy(d, g).wait_send()


def collect(n_sp, n_tp, part):
    experts, _, _, cap, width = part.shape
    groups = n_tp // pair_of(n_tp)
    sem = pltpu.SemaphoreType.DMA
    vmem = pl.BlockSpec(memory_space=pltpu.VMEM)
    piece = (experts, cap, width)
    return pl.pallas_call(
        functools.partial(collect_kernel, n_sp, n_tp),
        out_shape=jax.ShapeDtypeStruct((n_sp,) + piece, part.dtype),
        in_specs=[vmem],
        out_specs=vmem,
        scratch_shapes=[
            pltpu.VMEM((n_sp, groups) + piece, part.dtype),
            pltpu.VMEM((n_sp, groups) + piece, part.dtype),
            pltpu.VMEM((n_sp, groups) + piece, part.dtype),
            pltpu.VMEM((n_sp,) + piece, part.dtype),
            sem((n_sp, groups)),
            sem((n_sp, groups)),
            sem((n_sp, groups)),
            sem((n_sp, groups)),
            sem((n_sp,)),
            sem((n_sp,)),
        ],
        compiler_params=pltpu.CompilerParams(
            collective_id=2, has_side_effects=True, vmem_limit_bytes=VMEM_LIMIT
        ),
    )(part)


def experts_kernel(
    n_sp,
    n_tp,
    rows_ref,
    gate_hbm,
    up_hbm,
    down_hbm,
    out_ref,
    held,
    part,
    from_core,
    from_across,
    summed,
    total,
    gate_w,
    up_w,
    down_w,
    w_sem,
    own_sem,
    sp_send,
    sp_recv,
    y_send,
    y_recv,
    c_send,
    c_recv,
    rc_send,
    rc_recv,
    ry_send,
    ry_recv,
    rs_send,
    rs_recv,
):
    me, mt = lax.axis_index("sp"), lax.axis_index("tp")
    inner_sp = pair_of(n_sp)
    length = n_sp // inner_sp
    z, x = me // inner_sp, me % inner_sp
    inner, across, partner = tp_peers(n_tp)
    groups = n_tp // inner
    o, c = mt // inner, mt % inner
    experts, cap = rows_ref.shape[1], rows_ref.shape[2]
    weights = [
        pltpu.make_async_copy(src, dst, w_sem.at[k])
        for k, (src, dst) in enumerate(((gate_hbm, gate_w), (up_hbm, up_w), (down_hbm, down_w)))
    ]
    for copy in weights:
        copy.start()
    greet_all(n_sp, n_tp)

    def side(i):
        return (x + i % inner_sp) % inner_sp

    def to_of(i):
        return ((z + i // inner_sp) % length) * inner_sp + side(i)

    def from_of(i):
        return ((z + length - i // inner_sp) % length) * inner_sp + side(i)

    def span(t):
        return pl.ds(pl.multiple_of(t * cap, cap), cap)

    def remote(src, dst, send, recv, sp, tp):
        return pltpu.make_async_remote_copy(
            src_ref=src,
            dst_ref=dst,
            send_sem=send,
            recv_sem=recv,
            device_id={"sp": sp, "tp": tp},
            device_id_type=MESH,
        )

    def sp_copy(i):
        block = held.at[i, :, span(mt)]
        return remote(rows_ref.at[to_of(i)], block, sp_send.at[i], sp_recv.at[i], to_of(i), mt)

    def across_in(i, g, t):
        block = held.at[i, :, span(t)]
        return remote(block, block, y_send.at[g, i], y_recv.at[g, i], me, across[g - 1])

    def core_in(i, g, t):
        block = held.at[i, :, span(t)]
        return remote(block, block, c_send.at[g, i], c_recv.at[g, i], me, partner)

    def core_out(i, g):
        row = ((o + g) % groups) * inner + (inner - 1 - c)
        block = part.at[i, :, span(row)]
        return remote(
            block, from_core.at[i, g], rc_send.at[i, g], rc_recv.at[i, g], me, partner
        )

    def across_out(i, g):
        return remote(
            summed.at[i, g],
            from_across.at[i, g],
            ry_send.at[i, g],
            ry_recv.at[i, g],
            me,
            across[g - 1],
        )

    def sp_out(i):
        to = from_of(i)
        return remote(total.at[i], out_ref.at[me], rs_send.at[i], rs_recv.at[i], to, mt)

    def source(g):
        return ((o - g + groups) % groups) * inner + c

    for i in range(1, n_sp):
        sp_copy(i).start()
    own = pltpu.make_async_copy(rows_ref.at[me], held.at[0, :, span(mt)], own_sem)
    own.start()
    own.wait()

    def spread(i):
        @pl.when(i > 0)
        def _():
            sp_copy(i).wait_recv()

        for g in range(1, groups):
            across_in(i, g, mt).start()
        if inner == 2:
            core_in(i, 0, mt).start()

    def relay(i):
        for g in range(1, groups):
            across_in(i, g, source(g)).wait_recv()
            if inner == 2:
                core_in(i, g, source(g)).start()

    def compute(i):
        @pl.when(i == late)
        def _():
            for copy in weights:
                copy.wait()

        if inner == 2:
            for g in range(groups):
                core_in(i, g, source(g)).wait_recv()
        for e in range(experts):
            rows = held[i, e]
            gate = jnp.dot(rows, gate_w[e], preferred_element_type=jnp.float32)
            upper = jnp.dot(rows, up_w[e], preferred_element_type=jnp.float32)
            middle = (gate / (1.0 + jnp.exp(-gate)) * upper).astype(jnp.bfloat16)
            part[i, e] = jnp.dot(middle, down_w[e], preferred_element_type=jnp.float32).astype(
                part.dtype
            )
        if inner == 2:
            for g in list(range(1, groups)) + [0]:
                core_out(i, g).start()

    def pair_sum(i, g):
        row = ((o + g) % groups) * inner + c
        value = part[i, :, span(row), :].astype(jnp.float32)
        if inner == 2:
            core_out(i, g).wait_recv()
            value = value + from_core[i, g].astype(jnp.float32)
        return value

    def first(i):
        for g in range(1, groups):
            summed[i, g] = pair_sum(i, g).astype(summed.dtype)
            across_out(i, g).start()

    def second(i):
        value = pair_sum(i, 0)
        for g in range(1, groups):
            across_out(i, g).wait_recv()
            value = value + from_across[i, g].astype(jnp.float32)
        value = value.astype(total.dtype)

        @pl.when(i == 0)
        def _():
            out_ref[me] = value

        @pl.when(i > 0)
        def _():
            total[i] = value
            sp_out(i).start()

    late = inner_sp if length > 1 else 0

    def turned(stage):
        return lambda k: stage(jnp.where(k < n_sp - late, k + late, n_sp - 1 - k))

    stages = (spread, relay) + tuple(turned(stage) for stage in (compute, first, second))
    lags = (0, 1, 2 + late, 3 + late, 5 + late)

    def step(i, carry):
        for stage, lag in zip(stages, lags):

            @pl.when((i >= lag) & (i < n_sp + lag))
            def _():
                stage(i - lag)

        return carry

    lax.fori_loop(0, n_sp + lags[-1], step, 0)

    def drain(i, carry):
        @pl.when(i > 0)
        def _():
            sp_out(i).wait_recv()
            sp_out(i).wait_send()
            sp_copy(i).wait_send()

        for g in range(groups):
            if g:
                across_in(i, g, mt).wait_send()
                across_out(i, g).wait_send()
            if inner == 2:
                core_in(i, g, mt).wait_send()
                core_out(i, g).wait_send()
        return carry

    lax.fori_loop(0, n_sp, drain, 0)


def run_experts(n_sp, n_tp, rows, gate_weight, up_weight, down_weight):
    _, experts, cap, width = rows.shape
    groups = n_tp // pair_of(n_tp)
    dma = pltpu.SemaphoreType.DMA
    vmem = pl.BlockSpec(memory_space=pltpu.VMEM)
    hbm = pl.BlockSpec(memory_space=pl.ANY)
    piece = (experts, cap, width)
    return pl.pallas_call(
        functools.partial(experts_kernel, n_sp, n_tp),
        out_shape=jax.ShapeDtypeStruct(rows.shape, rows.dtype),
        in_specs=[vmem, hbm, hbm, hbm],
        out_specs=vmem,
        scratch_shapes=[
            pltpu.VMEM((n_sp, experts, n_tp * cap, width), rows.dtype),
            pltpu.VMEM((n_sp, experts, n_tp * cap, width), rows.dtype),
            pltpu.VMEM((n_sp, groups) + piece, rows.dtype),
            pltpu.VMEM((n_sp, groups) + piece, rows.dtype),
            pltpu.VMEM((n_sp, groups) + piece, rows.dtype),
            pltpu.VMEM((n_sp,) + piece, rows.dtype),
            pltpu.VMEM(gate_weight.shape, gate_weight.dtype),
            pltpu.VMEM(up_weight.shape, up_weight.dtype),
            pltpu.VMEM(down_weight.shape, down_weight.dtype),
            dma((3,)),
            dma,
            dma((n_sp,)),
            dma((n_sp,)),
            dma((groups, n_sp)),
            dma((groups, n_sp)),
            dma((groups, n_sp)),
            dma((groups, n_sp)),
            dma((n_sp, groups)),
            dma((n_sp, groups)),
            dma((n_sp, groups)),
            dma((n_sp, groups)),
            dma((n_sp,)),
            dma((n_sp,)),
        ],
        compiler_params=pltpu.CompilerParams(
            collective_id=3, has_side_effects=True, vmem_limit_bytes=VMEM_LIMIT
        ),
    )(rows, gate_weight, up_weight, down_weight)


def on_device(
    n_sp,
    n_tp,
    query_one,
    key_one,
    query_two,
    key_two,
    values,
    mix_lambda,
    head_gain,
    residual_in,
    out_weight,
    norm_gain,
    route_ids,
    route_logits,
    group_prob,
    gate_weight,
    up_weight,
    down_weight,
):
    token_heads = attend(
        n_sp,
        n_tp,
        key_one,
        key_two,
        values,
        query_one,
        query_two,
        mix_lambda,
        head_gain[None, :],
    )
    share = residual_in.shape[0]
    mix = jnp.dot(token_heads, out_weight, preferred_element_type=jnp.float32)
    hidden_f = (residual_in.astype(jnp.float32) + mix).astype(jnp.bfloat16).astype(jnp.float32)
    normed = (
        hidden_f
        * lax.rsqrt(jnp.mean(hidden_f * hidden_f, axis=-1, keepdims=True) + norm_epsilon)
        * norm_gain
    ).astype(jnp.bfloat16)
    width = normed.shape[1]
    top_count = route_ids.shape[1]
    local_experts = gate_weight.shape[0]
    expert_count = local_experts * n_sp
    capacity = max(2, 2 * share * top_count // expert_count)
    slots = expert_count * capacity
    flat_ids = route_ids.reshape(-1)
    one_hot = (flat_ids[:, None] == jnp.arange(expert_count, dtype=jnp.int32)[None, :]).astype(
        jnp.int32
    )
    earlier = jnp.cumsum(one_hot, axis=0) - one_hot
    rank = jnp.sum(earlier * one_hot, axis=1)
    slot_of = (flat_ids * capacity + rank).reshape(share, top_count)
    places = jnp.arange(slots, dtype=jnp.int32)
    table = sum(
        (places[:, None] == slot_of[None, :, k]).astype(jnp.bfloat16) for k in range(top_count)
    )
    outgoing = jnp.dot(table, normed, preferred_element_type=jnp.float32).astype(jnp.bfloat16)
    outgoing = outgoing.reshape(n_sp, local_experts, capacity, width)
    if capacity % 16 == 0:
        returned = run_experts(
            n_sp, n_tp, outgoing, gate_weight, up_weight, down_weight
        ).reshape(slots, width)
    else:
        everyone = dispatch(
            n_sp, n_tp, outgoing
        ).reshape(local_experts, n_tp * n_sp * capacity, width)
        gate = jnp.einsum("erd,edf->erf", everyone, gate_weight, preferred_element_type=jnp.float32)
        upper = jnp.einsum("erd,edf->erf", everyone, up_weight, preferred_element_type=jnp.float32)
        middle = (jax.nn.silu(gate) * upper).astype(jnp.bfloat16)
        part_sum = jnp.einsum(
            "erf,efd->erd", middle, down_weight, preferred_element_type=jnp.float32
        ).astype(jnp.bfloat16)
        returned = collect(
            n_sp, n_tp, part_sum.reshape(local_experts, n_tp, n_sp, capacity, width)
        ).reshape(slots, width)
    logits = [route_logits[:, k : k + 1] for k in range(top_count)]
    highest = functools.reduce(jnp.maximum, logits)
    powers = [jnp.exp(logit - highest) for logit in logits]
    route_weight = [power / sum(powers) * group_prob[:, None] for power in powers]
    spread = sum(
        jnp.where(places[None, :] == slot_of[:, k, None], route_weight[k], 0.0)
        for k in range(top_count)
    )
    high = spread.astype(jnp.bfloat16)
    low = (spread - high.astype(jnp.float32)).astype(jnp.bfloat16)
    both = jnp.dot(
        jnp.concatenate([high, low], axis=0), returned, preferred_element_type=jnp.float32
    )
    return (hidden_f + (both[:share] + both[share:])).astype(jnp.bfloat16)


def solution(mesh):
    in_specs = (
        P("sp", "tp"),
        P("sp", "tp"),
        P("sp", "tp"),
        P("sp", "tp"),
        P("sp", "tp"),
        P("tp"),
        P(),
        P(("sp", "tp"), None),
        P(),
        P(),
        P(("sp", "tp"), None),
        P(("sp", "tp"), None),
        P(("sp", "tp")),
        P("sp", None, "tp"),
        P("sp", None, "tp"),
        P("sp", "tp", None),
    )
    out_specs = P(("sp", "tp"), None)
    return jax.shard_map(
        functools.partial(on_device, mesh.shape["sp"], mesh.shape["tp"]),
        mesh=mesh,
        in_specs=in_specs,
        out_specs=out_specs,
        check_vma=False,
    )
```

profile of v0, /device:TPU:0, one launch (start us, length us, event | category | flops | bytes accessed | tf_op | source)
XLA Modules:
  0.0 112.9 jit_solution(7814334380116988433)
XLA Ops:
  0.0 0.0 copy-start
  0.0 0.8 fusion.24
  0.8 0.8 copy.23
  1.5 0.1 eq.72
  1.7 0.1 fusion.18
  1.8 0.2 reduce_window_sum.11
  2.0 0.2 select_reduce_fusion
  2.1 0.1 reduce_sum.21
  2.3 0.1 copy.24
  2.3 0.7 multiply_add_fusion
  3.1 0.1 fusion.17
  3.2 35.1 %shard_map.154 = bf16[64,1024]{1,0:T(8,128)(2,1)} custom-call(bf16[256,128]{1,0:T(8,128)(2,1)} %k1_ref.1, bf16[256,128]{1,0:T(8,128)(2,1)} %k2_ref.1, bf16[256,256]{1,0:T(8,128)(2,1)} %v_ref.1, bf16[256,128]{1,0:T(8,128)(2,1)} %q1_ref.1, bf16[256,128]{1,0:T(8,128)(2,1)} %q2_ref.1, f32[2]{0:T(128)} %lam_ref.1, f32[1,128]{1,0:T(1,128)} %bitcast.23), custom_call_target="tpu_custom_call" | custom-call | tf_op jit(solution)/shard_map/pallas_call | solution.py:315
  38.3 3.2 %multiply_reduce_fusion = (f32[64]{0:T(128)S(1)}, f32[64,2048]{1,0:T(8,128)S(1)}) fusion(bf16[64,1024]{1,0:T(8,128)(2,1)} %shard_map.154, bf16[1024,2048]{1,0:T(8,128)(2,1)} %param.24, bf16[64,2048]{1,0:T(8,128)(2,1)} %param.23), kind=kOutput, calls=%fused_computation.8 | convolution fusion | flops 269221824 | bytes 5112064 | tf_op jit(solution)/shard_map/dot_general | solution.py:892
  41.5 0.0 copy-done
  41.5 1.5 %convolution_convert_fusion = bf16[256,2048]{1,0:T(8,128)(2,1)} fusion(f32[64,2048]{1,0:T(8,128)S(1)} %get-tuple-element.12, f32[2048]{0:T(1024)S(1)} %copy-done, f32[64]{0:T(128)S(1)} %add_rsqrt_fusion, s32[64]{0:T(128)S(1)} %get-tuple-element.10, s32[64]{0:T(128)S(1)} %get-tuple-element.9), kind=kOutput, calls=%fused_computation | convolution fusion | flops 68157440 | bytes 1581824 | tf_op jit(solution)/shard_map/dot_general | solution.py:916
  43.0 67.5 %shard_map.155 = bf16[8,2,16,2048]{3,2,1,0:T(8,128)(2,1)} custom-call(bf16[8,2,16,2048]{3,2,1,0:T(8,128)(2,1)} %bitcast.21, bf16[2,2048,256]{2,1,0:T(8,128)(2,1)} %gate_hbm.1, bf16[2,2048,256]{2,1,0:T(8,128)(2,1)} %up_hbm.1, bf16[2,256,2048]{2,1,0:T(8,128)(2,1)} %down_hbm.1), custom_call_target="tpu_custom_call" | custom-call | tf_op jit(solution)/shard_map/pallas_call | solution.py:824
  110.5 1.5 %fusion.11 = f32[128,2048]{1,0:T(8,128)S(1)} fusion(bf16[256,2048]{1,0:T(8,128)(2,1)} %bitcast.22, bf16[64,256]{1,0:T(8,128)(2,1)S(1)} %get-tuple-element.6, bf16[64,256]{1,0:T(8,128)(2,1)S(1)} %get-tuple-element.5), kind=kOutput, calls=%fused_computation.16 | convolution fusion | flops 134348800 | bytes 2162688 | tf_op jit(solution)/shard_map/dot_general | solution.py:945
  112.1 0.8 fusion.3
  (2 shorter events, 0.0 us)
Async XLA Ops:
  0.0 41.5 %copy-start = (f32[2048]{0:T(1024)S(1)}, f32[2048]{0:T(1024)}, u32[]{:S(2)}) copy-start(f32[2048]{0:T(1024)} %param.25) | copy-start | bytes 24580
where the time goes:
time: 113 us
  Pallas kernels  103 us (91%)
  matrix products  6.24 us (6%)
  other arithmetic  2.79 us (2%)
    pallas_call x1, Pallas kernels, run_experts(): pl.pallas_call(functools.partial(experts_kernel, n_sp, n_tp), out_shape=j...  67.5 us
    pallas_call x1, Pallas kernels, attend(): pl.pallas_call(functools.partial(attend_kernel, n_sp, n_tp, vd), out_shap...  35.1 us
    dot_general x1, matrix products, on_device(): mix = jnp.dot(token_heads, out_weight, preferred_element_type=jnp.float32)  3.22 us

commit v1 on v0

--- a/solution.py
+++ b/solution.py
@@ -341,6 +341,340 @@
     )(k1, k2, v, q1, q2, lam, gain)
 
 
+def layered_kernel(
+    n_sp,
+    n_tp,
+    vd,
+    k1_ref,
+    k2_ref,
+    v_ref,
+    q1_ref,
+    q2_ref,
+    lam_ref,
+    gain_ref,
+    out_ref,
+    kv_out,
+    q_out,
+    held,
+    q_in,
+    qt,
+    m_ref,
+    l_ref,
+    acc_ref,
+    stage,
+    lam_mine,
+    lam_far,
+    first_send,
+    core_send,
+    side_send,
+    kv_recv,
+    q_recv,
+    lam_sem,
+    head_send,
+    head_recv,
+):
+    inner, pair = 2, 2
+    length = n_sp // inner
+    me, mt = lax.axis_index("sp"), lax.axis_index("tp")
+    z, x = me // inner, me % inner
+    y, c = mt // pair, mt % pair
+    rows, qk = q1_ref.shape[0], q1_ref.shape[1] // 2
+    keys = 2 * qk
+    scale = 1.0 / math.sqrt(qk)
+    exact = math.frexp(scale)[0] == 0.5
+    early, after = (scale, 1.0) if exact else (1.0, scale)
+    home = c == z // pair
+    partner = y * pair + (1 - c)
+    across = z * inner + (1 - x)
+
+    def spot(zz):
+        return zz * inner + x
+
+    barrier = pltpu.get_barrier_semaphore()
+    peers = [(spot(zz), t) for zz in range(length) for t in range(n_tp)]
+    for sp, tp in peers:
+
+        @pl.when((sp != me) | (tp != mt))
+        def _():
+            pl.semaphore_signal(
+                barrier, inc=1, device_id={"sp": sp, "tp": tp}, device_id_type=MESH
+            )
+
+    pl.semaphore_signal(barrier, inc=1, device_id={"sp": across, "tp": mt}, device_id_type=MESH)
+
+    for h in range(2):
+        at = slice(h * qk, (h + 1) * qk)
+        block = jnp.concatenate([k1_ref[:, at], k2_ref[:, at]], axis=1)
+        turned = jnp.concatenate(
+            [
+                v_ref[r : r + vd, h * vd : (h + 1) * vd].astype(jnp.float32).T
+                for r in range(0, rows, vd)
+            ],
+            axis=0,
+        ).astype(jnp.bfloat16)
+        query = jnp.concatenate([q1_ref[:, at], q2_ref[:, at]], axis=1) * jnp.bfloat16(early)
+        kv_out[h, :, 0:keys] = block
+        kv_out[h, :, keys : keys + vd] = turned
+        q_out[h] = query
+
+        @pl.when(z == pair * c + h)
+        def _():
+            held[z, 0, :, 0:keys] = block
+            held[z, 0, :, keys : keys + vd] = turned
+            q_in[h] = query
+
+    lam_mine[...] = jnp.full(lam_mine.shape, lam_ref[z % pair], jnp.float32)
+    m_ref[...] = jnp.full(m_ref.shape, -1e30, jnp.float32)
+    l_ref[...] = jnp.zeros(l_ref.shape, jnp.float32)
+    acc_ref[...] = jnp.zeros(acc_ref.shape, jnp.float32)
+    qt[...] = jnp.zeros(qt.shape, qt.dtype)
+    pl.semaphore_wait(barrier, len(peers))
+
+    def remote(src, dst, send, recv, sp, tp):
+        return pltpu.make_async_remote_copy(
+            src_ref=src,
+            dst_ref=dst,
+            send_sem=send,
+            recv_sem=recv,
+            device_id={"sp": sp, "tp": tp},
+            device_id_type=MESH,
+        )
+
+    def first_q(h):
+        return remote(
+            q_out.at[h],
+            q_in.at[z % pair],
+            first_send.at[0, h],
+            q_recv.at[z % pair],
+            spot(pair * c + h),
+            y * pair + z // pair,
+        )
+
+    def first_kv(h):
+        return remote(
+            kv_out.at[h],
+            held.at[z, 0],
+            first_send.at[1, h],
+            kv_recv.at[z, 0],
+            spot(pair * c + h),
+            y * pair + z // pair,
+        )
+
+    def to_core(zz, side):
+        block = held.at[zz, side]
+        return remote(block, block, core_send.at[zz, side], kv_recv.at[zz, side], me, partner)
+
+    def to_side(zz):
+        return remote(
+            held.at[zz, 0], held.at[zz, 1], side_send.at[zz], kv_recv.at[zz, 1], across, mt
+        )
+
+    lam_copy = remote(lam_mine, lam_far, lam_sem.at[0], lam_sem.at[1], me, partner)
+
+    def away(h):
+        return z != pair * c + h
+
+    order = [z, z + 1 - 2 * (z % pair), pair - z // pair, (length - 1) * (1 - z // pair)]
+
+    @pl.when(home)
+    def _():
+        to_side(z).start()
+        to_core(z, 0).start()
+
+    for h in range(2):
+
+        @pl.when(away(h))
+        def _():
+            first_q(h).start()
+
+    for h in range(2):
+
+        @pl.when(away(h))
+        def _():
+            first_kv(h).start()
+
+    lam_copy.start()
+
+    for g in range(2):
+
+        @pl.when((z != pair * c + g))
+        def _():
+            remote(
+                q_out.at[g], q_in.at[g], first_send.at[0, g], q_recv.at[g], me, mt
+            ).wait_recv()
+
+        turned = q_in[g].astype(jnp.float32).T.astype(jnp.bfloat16)
+        qt[0:qk, 2 * g * rows : (2 * g + 1) * rows] = turned[0:qk]
+        qt[qk:keys, (2 * g + 1) * rows : (2 * g + 2) * rows] = turned[qk:keys]
+
+    def absorb(zz, side):
+        block_keys = held[zz, side, :, 0:keys]
+        turned = jnp.concatenate(
+            [held[zz, side, r : r + vd, keys : keys + vd] for r in range(0, rows, vd)], axis=1
+        )
+        for part in range(4):
+            at = slice(part * rows, (part + 1) * rows)
+            scores = jnp.dot(block_keys, qt[:, at], preferred_element_type=jnp.float32)
+            if after != 1.0:
+                scores = scores * after
+            old = m_ref[:, at]
+            new = jnp.maximum(old, jnp.max(scores, axis=0, keepdims=True))
+            shrink = jnp.exp(old - new)
+            expo = jnp.exp(scores - new)
+            m_ref[:, at] = new
+            l_ref[:, at] = l_ref[:, at] * shrink + jnp.sum(expo, axis=0, keepdims=True)
+            acc_ref[:, at] = acc_ref[:, at] * shrink + jnp.dot(
+                turned, expo.astype(jnp.bfloat16), preferred_element_type=jnp.float32
+            )
+
+    def take(zz):
+        direct = zz // pair == c
+
+        @pl.when((zz != z) | jnp.logical_not(home))
+        def _():
+            to_core(zz, 0).wait_recv()
+
+        @pl.when(direct & (zz != z))
+        def _():
+            to_side(zz).start()
+            to_core(zz, 0).start()
+
+        absorb(zz, 0)
+        to_core(zz, 1).wait_recv()
+
+        @pl.when(direct)
+        def _():
+            to_core(zz, 1).start()
+
+        absorb(zz, 1)
+
+    def step(n, carry):
+        take(jnp.where(n == 0, order[0], jnp.where(n == 1, order[1], jnp.where(n == 2, order[2], order[3]))))
+        return carry
+
+    lax.fori_loop(0, length, step, 0)
+
+    share = rows // n_tp
+    lam_copy.wait()
+    lam = jnp.where(home, lam_mine[0:1, 0:1], lam_far[0:1, 0:1])
+    head = y * length + z
+    columns = pl.ds(pl.multiple_of(head * vd, vd), vd)
+
+    def piece(g, t):
+        to = (mt + t) % n_tp
+        span = pl.ds(pl.multiple_of(to * share, share), share)
+        return remote(
+            stage.at[g, span],
+            out_ref.at[:, columns],
+            head_send.at[g, t],
+            head_recv.at[head],
+            spot(pair * c + g),
+            to,
+        )
+
+    def own(g):
+        return z == pair * c + g
+
+    for g in (1, 0):
+        reads = []
+        for which in range(2):
+            at = slice((2 * g + which) * rows, (2 * g + which + 1) * rows)
+            reads.append(acc_ref[:, at] / l_ref[:, at])
+        combined = reads[0] - lam * reads[1]
+        combined = combined * lax.rsqrt(
+            jnp.mean(combined * combined, axis=0, keepdims=True) + norm_epsilon
+        )
+        stage[g] = (combined.T * gain_ref[...]).astype(jnp.bfloat16)
+        for t in range(1, n_tp):
+            piece(g, t).start()
+
+        @pl.when(own(g))
+        def _():
+            out_ref[:, columns] = stage[g, pl.ds(pl.multiple_of(mt * share, share), share), :]
+
+        @pl.when(jnp.logical_not(own(g)))
+        def _():
+            piece(g, 0).start()
+
+    def head_copy(hd):
+        at = pl.ds(pl.multiple_of(hd * vd, vd), vd)
+        return remote(
+            stage.at[0, 0:share], out_ref.at[:, at], head_send.at[0, 0], head_recv.at[hd], me, mt
+        )
+
+    for hd in range(2 * n_tp):
+
+        @pl.when((hd != head) | jnp.logical_not(home))
+        def _():
+            head_copy(hd).wait_recv()
+
+    for g in range(2):
+        for t in range(1, n_tp):
+            piece(g, t).wait_send()
+
+        @pl.when(jnp.logical_not(own(g)))
+        def _():
+            piece(g, 0).wait_send()
+
+        @pl.when(away(g))
+        def _():
+            first_q(g).wait_send()
+            first_kv(g).wait_send()
+
+    for zz in range(length):
+
+        @pl.when(c == zz // pair)
+        def _():
+            to_side(zz).wait_send()
+            to_core(zz, 0).wait_send()
+            to_core(zz, 1).wait_send()
+
+
+def layered(n_sp, n_tp, k1, k2, v, q1, q2, lam, gain):
+    rows = q1.shape[0]
+    length = n_sp // 2
+    vd = v.shape[1] // 2
+    keys = q1.shape[1]
+    cols = keys + vd
+    vmem = pl.BlockSpec(memory_space=pltpu.VMEM)
+    dma = pltpu.SemaphoreType.DMA
+    return pl.pallas_call(
+        functools.partial(layered_kernel, n_sp, n_tp, vd),
+        out_shape=jax.ShapeDtypeStruct((rows // n_tp, n_tp * 2 * vd), jnp.bfloat16),
+        in_specs=[vmem] * 5 + [pl.BlockSpec(memory_space=pltpu.SMEM), vmem],
+        out_specs=vmem,
+        scratch_shapes=[
+            pltpu.VMEM((2, rows, cols), jnp.bfloat16),
+            pltpu.VMEM((2, rows, keys), jnp.bfloat16),
+            pltpu.VMEM((length, 2, rows, cols), jnp.bfloat16),
+            pltpu.VMEM((2, rows, keys), jnp.bfloat16),
+            pltpu.VMEM((keys, 4 * rows), jnp.bfloat16),
+            pltpu.VMEM((1, 4 * rows), jnp.float32),
+            pltpu.VMEM((1, 4 * rows), jnp.float32),
+            pltpu.VMEM((vd, 4 * rows), jnp.float32),
+            pltpu.VMEM((2, rows, vd), jnp.bfloat16),
+            pltpu.VMEM((8, 128), jnp.float32),
+            pltpu.VMEM((8, 128), jnp.float32),
+            dma((2, 2)),
+            dma((length, 2)),
+            dma((length,)),
+            dma((length, 2)),
+            dma((2,)),
+            dma((2,)),
+            dma((2, n_tp)),
+            dma((2 * n_tp,)),
+        ],
+        compiler_params=pltpu.CompilerParams(
+            collective_id=4, has_side_effects=True, vmem_limit_bytes=VMEM_LIMIT
+        ),
+    )(k1, k2, v, q1, q2, lam, gain)
+
+
+def layers_fit(n_sp, n_tp, rows, vd, keys, heads):
+    square = heads == 2 and n_sp == 8 and pair_of(n_tp) == 2
+    return square and rows % (2 * vd) == 0 and rows // vd * vd == rows and vd == keys
+
+
 def tp_peers(n_tp):
     inner = pair_of(n_tp)
     mt = lax.axis_index("tp")
@@ -877,7 +1211,15 @@
     up_weight,
     down_weight,
 ):
-    token_heads = attend(
+    fits = layers_fit(
+        n_sp,
+        n_tp,
+        query_one.shape[0],
+        values.shape[1] // 2,
+        query_one.shape[1],
+        mix_lambda.shape[0],
+    )
+    token_heads = (layered if fits else attend)(
         n_sp,
         n_tp,
         key_one,

time: 113 us -> 115 us (1.018)
  Pallas kernels: 103 us -> 105 us
    pallas_call x1, Pallas kernels: 67.5 us -> 69.5 us  [run_experts(): pl.pallas_call(functools.partial(experts_kernel, n_sp, n_tp), out_shape=j...]
where the time goes in v1:
time: 115 us
  Pallas kernels  105 us (91%)
  matrix products  6.23 us (5%)
  other arithmetic  2.79 us (2%)
    pallas_call x1, Pallas kernels, run_experts(): pl.pallas_call(functools.partial(experts_kernel, n_sp, n_tp), out_shape=j...  69.5 us
    pallas_call x1, Pallas kernels, layered(): pl.pallas_call(functools.partial(layered_kernel, n_sp, n_tp, vd), out_sha...  35.4 us
    dot_general x1, matrix products, on_device(): mix = jnp.dot(token_heads, out_weight, preferred_element_type=jnp.float32)  3.21 us

profile of v1, /device:TPU:0, one launch (start us, length us, event | category | flops | bytes accessed | tf_op | source)
XLA Modules:
  0.0 115.2 jit_solution(7804603968490328708)
XLA Ops:
  0.0 0.0 copy-start
  0.0 0.8 fusion.24
  0.8 0.8 copy.23
  1.5 0.1 eq.72
  1.7 0.1 fusion.18
  1.8 0.2 reduce_window_sum.11
  2.0 0.2 select_reduce_fusion
  2.1 0.1 reduce_sum.21
  2.3 0.1 copy.24
  2.3 0.7 multiply_add_fusion
  3.1 0.1 fusion.17
  3.2 35.4 %shard_map.154 = bf16[64,1024]{1,0:T(8,128)(2,1)} custom-call(bf16[256,128]{1,0:T(8,128)(2,1)} %k1_ref.1, bf16[256,128]{1,0:T(8,128)(2,1)} %k2_ref.1, bf16[256,256]{1,0:T(8,128)(2,1)} %v_ref.1, bf16[256,128]{1,0:T(8,128)(2,1)} %q1_ref.1, bf16[256,128]{1,0:T(8,128)(2,1)} %q2_ref.1, f32[2]{0:T(128)} %lam_ref.1, f32[1,128]{1,0:T(1,128)} %bitcast.23), custom_call_target="tpu_custom_call" | custom-call | tf_op jit(solution)/shard_map/pallas_call | solution.py:641
  38.6 3.2 %multiply_reduce_fusion = (f32[64]{0:T(128)S(1)}, f32[64,2048]{1,0:T(8,128)S(1)}) fusion(bf16[64,1024]{1,0:T(8,128)(2,1)} %shard_map.154, bf16[1024,2048]{1,0:T(8,128)(2,1)} %param.24, bf16[64,2048]{1,0:T(8,128)(2,1)} %param.23), kind=kOutput, calls=%fused_computation.8 | convolution fusion | flops 269221824 | bytes 5112064 | tf_op jit(solution)/shard_map/dot_general | solution.py:1234
  41.8 0.0 copy-done
  41.9 1.5 %convolution_convert_fusion = bf16[256,2048]{1,0:T(8,128)(2,1)} fusion(f32[64,2048]{1,0:T(8,128)S(1)} %get-tuple-element.12, f32[2048]{0:T(1024)S(1)} %copy-done, f32[64]{0:T(128)S(1)} %add_rsqrt_fusion, s32[64]{0:T(128)S(1)} %get-tuple-element.10, s32[64]{0:T(128)S(1)} %get-tuple-element.9), kind=kOutput, calls=%fused_computation | convolution fusion | flops 68157440 | bytes 1581824 | tf_op jit(solution)/shard_map/dot_general | solution.py:1258
  43.3 69.5 %shard_map.155 = bf16[8,2,16,2048]{3,2,1,0:T(8,128)(2,1)} custom-call(bf16[8,2,16,2048]{3,2,1,0:T(8,128)(2,1)} %bitcast.21, bf16[2,2048,256]{2,1,0:T(8,128)(2,1)} %gate_hbm.1, bf16[2,2048,256]{2,1,0:T(8,128)(2,1)} %up_hbm.1, bf16[2,256,2048]{2,1,0:T(8,128)(2,1)} %down_hbm.1), custom_call_target="tpu_custom_call" | custom-call | tf_op jit(solution)/shard_map/pallas_call | solution.py:1158
  112.9 1.5 %fusion.11 = f32[128,2048]{1,0:T(8,128)S(1)} fusion(bf16[256,2048]{1,0:T(8,128)(2,1)} %bitcast.22, bf16[64,256]{1,0:T(8,128)(2,1)S(1)} %get-tuple-element.6, bf16[64,256]{1,0:T(8,128)(2,1)S(1)} %get-tuple-element.5), kind=kOutput, calls=%fused_computation.16 | convolution fusion | flops 134348800 | bytes 2162688 | tf_op jit(solution)/shard_map/dot_general | solution.py:1287
  114.4 0.8 fusion.3
  (2 shorter events, 0.0 us)
Async XLA Ops:
  0.0 41.9 %copy-start = (f32[2048]{0:T(1024)S(1)}, f32[2048]{0:T(1024)}, u32[]{:S(2)}) copy-start(f32[2048]{0:T(1024)} %param.25) | copy-start | bytes 24580

commit v2 on v0

--- a/solution.py
+++ b/solution.py
@@ -1,5 +1,6 @@
 import functools
 import math
+import types
 
 import jax
 import jax.numpy as jnp
@@ -598,65 +599,52 @@
     )(part)
 
 
-def experts_kernel(
-    n_sp,
-    n_tp,
-    rows_ref,
-    gate_hbm,
-    up_hbm,
-    down_hbm,
-    out_ref,
-    held,
-    part,
-    from_core,
-    from_across,
-    summed,
-    total,
-    gate_w,
-    up_w,
-    down_w,
-    w_sem,
-    own_sem,
-    sp_send,
-    sp_recv,
-    y_send,
-    y_recv,
-    c_send,
-    c_recv,
-    rc_send,
-    rc_recv,
-    ry_send,
-    ry_recv,
-    rs_send,
-    rs_recv,
-):
+def attention_phase(n_sp, n_tp, r, arrived, filler):
+    inner, pair = 2, 2
+    length = n_sp // inner
     me, mt = lax.axis_index("sp"), lax.axis_index("tp")
-    inner_sp = pair_of(n_sp)
-    length = n_sp // inner_sp
-    z, x = me // inner_sp, me % inner_sp
-    inner, across, partner = tp_peers(n_tp)
-    groups = n_tp // inner
-    o, c = mt // inner, mt % inner
-    experts, cap = rows_ref.shape[1], rows_ref.shape[2]
-    weights = [
-        pltpu.make_async_copy(src, dst, w_sem.at[k])
-        for k, (src, dst) in enumerate(((gate_hbm, gate_w), (up_hbm, up_w), (down_hbm, down_w)))
-    ]
-    for copy in weights:
-        copy.start()
-    greet_all(n_sp, n_tp)
-
-    def side(i):
-        return (x + i % inner_sp) % inner_sp
-
-    def to_of(i):
-        return ((z + i // inner_sp) % length) * inner_sp + side(i)
-
-    def from_of(i):
-        return ((z + length - i // inner_sp) % length) * inner_sp + side(i)
-
-    def span(t):
-        return pl.ds(pl.multiple_of(t * cap, cap), cap)
+    z, x = me // inner, me % inner
+    y, c = mt // pair, mt % pair
+    rows, qk = r.q1_ref.shape[0], r.q1_ref.shape[1] // 2
+    vd = r.v_ref.shape[1] // 2
+    keys = 2 * qk
+    scale = 1.0 / math.sqrt(qk)
+    exact = math.frexp(scale)[0] == 0.5
+    early, after = (scale, 1.0) if exact else (1.0, scale)
+    home = c == z // pair
+    partner = y * pair + (1 - c)
+    across = z * inner + (1 - x)
+
+    def spot(zz):
+        return zz * inner + x
+
+    for h in range(2):
+        at = slice(h * qk, (h + 1) * qk)
+        block = jnp.concatenate([r.k1_ref[:, at], r.k2_ref[:, at]], axis=1)
+        turned = jnp.concatenate(
+            [
+                r.v_ref[base : base + vd, h * vd : (h + 1) * vd].astype(jnp.float32).T
+                for base in range(0, rows, vd)
+            ],
+            axis=0,
+        ).astype(jnp.bfloat16)
+        query = jnp.concatenate([r.q1_ref[:, at], r.q2_ref[:, at]], axis=1) * jnp.bfloat16(early)
+        r.kv_out[h, :, 0:keys] = block
+        r.kv_out[h, :, keys : keys + vd] = turned
+        r.q_out[h] = query
+
+        @pl.when(z == pair * c + h)
+        def _():
+            r.held[z, 0, :, 0:keys] = block
+            r.held[z, 0, :, keys : keys + vd] = turned
+            r.q_in[h] = query
+
+    r.lam_mine[...] = jnp.full(r.lam_mine.shape, r.lam_ref[z % pair], jnp.float32)
+    r.m_ref[...] = jnp.full(r.m_ref.shape, -1e30, jnp.float32)
+    r.l_ref[...] = jnp.zeros(r.l_ref.shape, jnp.float32)
+    r.acc_ref[...] = jnp.zeros(r.acc_ref.shape, jnp.float32)
+    r.qt[...] = jnp.zeros(r.qt.shape, r.qt.dtype)
+    arrived()
 
     def remote(src, dst, send, recv, sp, tp):
         return pltpu.make_async_remote_copy(
@@ -668,47 +656,326 @@
             device_id_type=MESH,
         )
 
+    def first_q(h):
+        return remote(
+            r.q_out.at[h],
+            r.q_in.at[z % pair],
+            r.first_send.at[0, h],
+            r.q_recv.at[z % pair],
+            spot(pair * c + h),
+            y * pair + z // pair,
+        )
+
+    def first_kv(h):
+        return remote(
+            r.kv_out.at[h],
+            r.held.at[z, 0],
+            r.first_send.at[1, h],
+            r.kv_recv.at[z, 0],
+            spot(pair * c + h),
+            y * pair + z // pair,
+        )
+
+    def to_core(zz, side):
+        block = r.held.at[zz, side]
+        return remote(block, block, r.core_send.at[zz, side], r.kv_recv.at[zz, side], me, partner)
+
+    def to_side(zz):
+        return remote(
+            r.held.at[zz, 0], r.held.at[zz, 1], r.side_send.at[zz], r.kv_recv.at[zz, 1], across, mt
+        )
+
+    lam_copy = remote(r.lam_mine, r.lam_far, r.lam_sem.at[0], r.lam_sem.at[1], me, partner)
+
+    def away(h):
+        return z != pair * c + h
+
+    order = [z, z + 1 - 2 * (z % pair), pair - z // pair, (length - 1) * (1 - z // pair)]
+
+    @pl.when(home)
+    def _():
+        to_side(z).start()
+        to_core(z, 0).start()
+
+    for h in range(2):
+
+        @pl.when(away(h))
+        def _():
+            first_q(h).start()
+
+    for h in range(2):
+
+        @pl.when(away(h))
+        def _():
+            first_kv(h).start()
+
+    lam_copy.start()
+    filler()
+
+    for g in range(2):
+
+        @pl.when((z != pair * c + g))
+        def _():
+            remote(
+                r.q_out.at[g], r.q_in.at[g], r.first_send.at[0, g], r.q_recv.at[g], me, mt
+            ).wait_recv()
+
+        turned = r.q_in[g].astype(jnp.float32).T.astype(jnp.bfloat16)
+        r.qt[0:qk, 2 * g * rows : (2 * g + 1) * rows] = turned[0:qk]
+        r.qt[qk:keys, (2 * g + 1) * rows : (2 * g + 2) * rows] = turned[qk:keys]
+
+    def absorb(zz, side):
+        block_keys = r.held[zz, side, :, 0:keys]
+        turned = jnp.concatenate(
+            [r.held[zz, side, base : base + vd, keys : keys + vd] for base in range(0, rows, vd)], axis=1
+        )
+        for part in range(4):
+            at = slice(part * rows, (part + 1) * rows)
+            scores = jnp.dot(block_keys, r.qt[:, at], preferred_element_type=jnp.float32)
+            if after != 1.0:
+                scores = scores * after
+            old = r.m_ref[:, at]
+            new = jnp.maximum(old, jnp.max(scores, axis=0, keepdims=True))
+            shrink = jnp.exp(old - new)
+            expo = jnp.exp(scores - new)
+            r.m_ref[:, at] = new
+            r.l_ref[:, at] = r.l_ref[:, at] * shrink + jnp.sum(expo, axis=0, keepdims=True)
+            r.acc_ref[:, at] = r.acc_ref[:, at] * shrink + jnp.dot(
+                turned, expo.astype(jnp.bfloat16), preferred_element_type=jnp.float32
+            )
+
+    near_first = ((0, 0), (0, 1), (1, 0), (1, 1), (2, 0), (3, 0), (2, 1), (3, 1))
+    far_first = ((0, 0), (0, 1), (1, 0), (2, 0), (1, 1), (3, 0), (2, 1), (3, 1))
+
+    def pick(values, n):
+        result = values[0]
+        for k in range(1, len(values)):
+            result = jnp.where(n == k, values[k], result)
+        return result
+
+    def step(n, carry):
+        at_home = [pick([p[i] for p in near_first], n) for i in range(2)]
+        at_far = [pick([p[i] for p in far_first], n) for i in range(2)]
+        zz = pick(order, jnp.where(home, at_home[0], at_far[0]))
+        side = jnp.where(home, at_home[1], at_far[1])
+        direct = zz // pair == c
+        local = home & (n == 0)
+
+        @pl.when(jnp.logical_not(local))
+        def _():
+            to_core(zz, side).wait_recv()
+
+            @pl.when(direct & (side == 0))
+            def _():
+                to_side(zz).start()
+
+            @pl.when(direct)
+            def _():
+                to_core(zz, side).start()
+
+        absorb(zz, side)
+        return carry
+
+    lax.fori_loop(0, 2 * length, step, 0)
+
+    share = rows // n_tp
+    lam_copy.wait()
+    lam = jnp.where(home, r.lam_mine[0:1, 0:1], r.lam_far[0:1, 0:1])
+    head = y * length + z
+    columns = pl.ds(pl.multiple_of(head * vd, vd), vd)
+
+    def piece(g, t):
+        to = (mt + t) % n_tp
+        span = pl.ds(pl.multiple_of(to * share, share), share)
+        return remote(
+            r.stage.at[g, span],
+            r.token_ref.at[:, columns],
+            r.head_send.at[g, t],
+            r.head_recv.at[head],
+            spot(pair * c + g),
+            to,
+        )
+
+    def own(g):
+        return z == pair * c + g
+
+    for g in (1, 0):
+        reads = []
+        for which in range(2):
+            at = slice((2 * g + which) * rows, (2 * g + which + 1) * rows)
+            reads.append(r.acc_ref[:, at] / r.l_ref[:, at])
+        combined = reads[0] - lam * reads[1]
+        combined = combined * lax.rsqrt(
+            jnp.mean(combined * combined, axis=0, keepdims=True) + norm_epsilon
+        )
+        r.stage[g] = (combined.T * r.gain_ref[...]).astype(jnp.bfloat16)
+        for t in range(1, n_tp):
+            piece(g, t).start()
+
+        @pl.when(own(g))
+        def _():
+            r.token_ref[:, columns] = r.stage[g, pl.ds(pl.multiple_of(mt * share, share), share), :]
+
+        @pl.when(jnp.logical_not(own(g)))
+        def _():
+            piece(g, 0).start()
+
+    def head_copy(hd):
+        at = pl.ds(pl.multiple_of(hd * vd, vd), vd)
+        return remote(
+            r.stage.at[0, 0:share], r.token_ref.at[:, at], r.head_send.at[0, 0], r.head_recv.at[hd], me, mt
+        )
+
+    for hd in range(2 * n_tp):
+
+        @pl.when((hd != head) | jnp.logical_not(home))
+        def _():
+            head_copy(hd).wait_recv()
+
+    for g in range(2):
+        for t in range(1, n_tp):
+            piece(g, t).wait_send()
+
+        @pl.when(jnp.logical_not(own(g)))
+        def _():
+            piece(g, 0).wait_send()
+
+        @pl.when(away(g))
+        def _():
+            first_q(g).wait_send()
+            first_kv(g).wait_send()
+
+    for zz in range(length):
+
+        @pl.when(c == zz // pair)
+        def _():
+            to_side(zz).wait_send()
+            to_core(zz, 0).wait_send()
+            to_core(zz, 1).wait_send()
+
+
+def routing_tables(r, experts_in_all, cap):
+    ids = r.ids_ref[...].astype(jnp.float32)
+    top, share = ids.shape
+    names = lax.broadcasted_iota(jnp.int32, (experts_in_all, share), 0).astype(jnp.float32)
+    before = lax.broadcasted_iota(jnp.int32, (share, share), 0)
+    before = before < lax.broadcasted_iota(jnp.int32, (share, share), 1)
+    before = before.astype(jnp.float32).astype(jnp.bfloat16)
+    taken = jnp.zeros((experts_in_all, 1), jnp.float32)
+    places = lax.broadcasted_iota(jnp.int32, (experts_in_all * cap, share), 0).astype(jnp.float32)
+    logits = [r.logits_ref[k : k + 1, :] for k in range(top)]
+    highest = functools.reduce(jnp.maximum, logits)
+    powers = [jnp.exp(logit - highest) for logit in logits]
+    total = sum(powers)
+    table = jnp.zeros(places.shape, jnp.float32)
+    spread = jnp.zeros(places.shape, jnp.float32)
+    for k in range(top):
+        hit = (names == ids[k : k + 1, :]).astype(jnp.float32)
+        earlier = jnp.dot(hit.astype(jnp.bfloat16), before, preferred_element_type=jnp.float32)
+        rank = jnp.sum(hit * (earlier + taken), axis=0, keepdims=True)
+        taken = taken + jnp.sum(hit, axis=1, keepdims=True)
+        placed = (places == ids[k : k + 1, :] * cap + rank).astype(jnp.float32)
+        table = table + placed
+        spread = spread + placed * (powers[k] / total * r.prob_ref[...])
+    r.table[...] = table.astype(jnp.bfloat16)
+    turned = spread.T
+    high = turned.astype(jnp.bfloat16)
+    r.spread[0:share] = high
+    r.spread[share : 2 * share] = (turned - high.astype(jnp.float32)).astype(jnp.bfloat16)
+
+
+def token_phase(r, wait_weights):
+    share, width = r.residual.shape
+    tile = math.gcd(width, 512)
+    columns = [slice(n, n + tile) for n in range(0, width, tile)]
+    wait_weights()
+    square = jnp.zeros((share, 1), jnp.float32)
+    for at in columns:
+        mix = jnp.dot(r.token_ref[...], r.out_w[:, at], preferred_element_type=jnp.float32)
+        hidden = (r.residual[:, at].astype(jnp.float32) + mix).astype(jnp.bfloat16)
+        r.hidden[:, at] = hidden
+        hidden = hidden.astype(jnp.float32)
+        square = square + jnp.sum(hidden * hidden, axis=1, keepdims=True)
+    factor = lax.rsqrt(square / width + norm_epsilon)
+    n_sp, experts, cap = r.outgoing.shape[:3]
+    for at in columns:
+        normed = r.hidden[:, at].astype(jnp.float32) * factor * r.norm_ref[:, at]
+        rows = jnp.dot(
+            r.table[...], normed.astype(jnp.bfloat16), preferred_element_type=jnp.float32
+        ).astype(jnp.bfloat16)
+        r.outgoing[:, :, :, at] = rows.reshape(n_sp, experts, cap, tile)
+
+
+def expert_phase(n_sp, n_tp, r, weights):
+    me, mt = lax.axis_index("sp"), lax.axis_index("tp")
+    inner_sp = 2
+    z, x = me // inner_sp, me % inner_sp
+    inner, across, partner = tp_peers(n_tp)
+    groups = n_tp // inner
+    o, c = mt // inner, mt % inner
+    _, experts, cap, _ = r.outgoing.shape
+
+    def flip(number, by):
+        low = (number % 2 + by % 2) % 2
+        return (number // 2 + by // 2) % 2 * 2 + low
+
+    def peer_of(i):
+        return flip(z, i // inner_sp) * inner_sp + flip(x, i % inner_sp)
+
+    def span(t):
+        return pl.ds(pl.multiple_of(t * cap, cap), cap)
+
+    def remote(src, dst, send, recv, sp, tp):
+        return pltpu.make_async_remote_copy(
+            src_ref=src,
+            dst_ref=dst,
+            send_sem=send,
+            recv_sem=recv,
+            device_id={"sp": sp, "tp": tp},
+            device_id_type=MESH,
+        )
+
     def sp_copy(i):
-        block = held.at[i, :, span(mt)]
-        return remote(rows_ref.at[to_of(i)], block, sp_send.at[i], sp_recv.at[i], to_of(i), mt)
+        to = peer_of(i)
+        block = r.rows.at[i, :, span(mt)]
+        return remote(r.outgoing.at[to], block, r.sp_send.at[i], r.sp_recv.at[i], to, mt)
 
     def across_in(i, g, t):
-        block = held.at[i, :, span(t)]
-        return remote(block, block, y_send.at[g, i], y_recv.at[g, i], me, across[g - 1])
+        block = r.rows.at[i, :, span(t)]
+        return remote(block, block, r.y_send.at[g, i], r.y_recv.at[g, i], me, across[g - 1])
 
     def core_in(i, g, t):
-        block = held.at[i, :, span(t)]
-        return remote(block, block, c_send.at[g, i], c_recv.at[g, i], me, partner)
+        block = r.rows.at[i, :, span(t)]
+        return remote(block, block, r.c_send.at[g, i], r.c_recv.at[g, i], me, partner)
 
     def core_out(i, g):
         row = ((o + g) % groups) * inner + (inner - 1 - c)
-        block = part.at[i, :, span(row)]
+        block = r.part.at[i, :, span(row)]
         return remote(
-            block, from_core.at[i, g], rc_send.at[i, g], rc_recv.at[i, g], me, partner
+            block, r.from_core.at[i, g], r.rc_send.at[i, g], r.rc_recv.at[i, g], me, partner
         )
 
     def across_out(i, g):
         return remote(
-            summed.at[i, g],
-            from_across.at[i, g],
-            ry_send.at[i, g],
-            ry_recv.at[i, g],
+            r.summed.at[i, g],
+            r.from_across.at[i, g],
+            r.ry_send.at[i, g],
+            r.ry_recv.at[i, g],
             me,
             across[g - 1],
         )
 
     def sp_out(i):
-        to = from_of(i)
-        return remote(total.at[i], out_ref.at[me], rs_send.at[i], rs_recv.at[i], to, mt)
+        return remote(
+            r.total.at[i], r.returned.at[me], r.rs_send.at[i], r.rs_recv.at[i], peer_of(i), mt
+        )
 
     def source(g):
         return ((o - g + groups) % groups) * inner + c
 
     for i in range(1, n_sp):
         sp_copy(i).start()
-    own = pltpu.make_async_copy(rows_ref.at[me], held.at[0, :, span(mt)], own_sem)
-    own.start()
-    own.wait()
+    r.rows[0, :, span(mt), :] = r.outgoing[me]
 
     def spread(i):
         @pl.when(i > 0)
@@ -717,72 +984,71 @@
 
         for g in range(1, groups):
             across_in(i, g, mt).start()
-        if inner == 2:
-            core_in(i, 0, mt).start()
+        core_in(i, 0, mt).start()
 
     def relay(i):
         for g in range(1, groups):
             across_in(i, g, source(g)).wait_recv()
-            if inner == 2:
-                core_in(i, g, source(g)).start()
+            core_in(i, g, source(g)).start()
+
+    half = n_sp // 2
 
     def compute(i):
-        @pl.when(i == late)
+        @pl.when(i == half)
         def _():
             for copy in weights:
                 copy.wait()
 
-        if inner == 2:
-            for g in range(groups):
-                core_in(i, g, source(g)).wait_recv()
+        for g in range(groups):
+            core_in(i, g, source(g)).wait_recv()
         for e in range(experts):
-            rows = held[i, e]
-            gate = jnp.dot(rows, gate_w[e], preferred_element_type=jnp.float32)
-            upper = jnp.dot(rows, up_w[e], preferred_element_type=jnp.float32)
+            rows = r.rows[i, e]
+            gate = jnp.dot(rows, r.gate_w[e], preferred_element_type=jnp.float32)
+            upper = jnp.dot(rows, r.up_w[e], preferred_element_type=jnp.float32)
             middle = (gate / (1.0 + jnp.exp(-gate)) * upper).astype(jnp.bfloat16)
-            part[i, e] = jnp.dot(middle, down_w[e], preferred_element_type=jnp.float32).astype(
-                part.dtype
+            r.part[i, e] = jnp.dot(middle, r.down_w[e], preferred_element_type=jnp.float32).astype(
+                r.part.dtype
             )
-        if inner == 2:
-            for g in list(range(1, groups)) + [0]:
-                core_out(i, g).start()
+        for g in list(range(1, groups)) + [0]:
+            core_out(i, g).start()
 
     def pair_sum(i, g):
         row = ((o + g) % groups) * inner + c
-        value = part[i, :, span(row), :].astype(jnp.float32)
-        if inner == 2:
-            core_out(i, g).wait_recv()
-            value = value + from_core[i, g].astype(jnp.float32)
-        return value
+        value = r.part[i, :, span(row), :].astype(jnp.float32)
+        core_out(i, g).wait_recv()
+        return value + r.from_core[i, g].astype(jnp.float32)
 
     def first(i):
         for g in range(1, groups):
-            summed[i, g] = pair_sum(i, g).astype(summed.dtype)
+            r.summed[i, g] = pair_sum(i, g).astype(r.summed.dtype)
             across_out(i, g).start()
 
     def second(i):
         value = pair_sum(i, 0)
         for g in range(1, groups):
             across_out(i, g).wait_recv()
-            value = value + from_across[i, g].astype(jnp.float32)
-        value = value.astype(total.dtype)
+            value = value + r.from_across[i, g].astype(jnp.float32)
+        value = value.astype(r.total.dtype)
 
         @pl.when(i == 0)
         def _():
-            out_ref[me] = value
+            r.returned[me] = value
 
         @pl.when(i > 0)
         def _():
-            total[i] = value
+            r.total[i] = value
             sp_out(i).start()
 
-    late = inner_sp if length > 1 else 0
+    def far_first(k):
+        near = n_sp - 1 - k
+        near = jnp.where(near > 1, half // 2 + n_sp - 1 - half - near, near)
+        return jnp.where(k < half, k + half, near)
 
     def turned(stage):
-        return lambda k: stage(jnp.where(k < n_sp - late, k + late, n_sp - 1 - k))
+        return lambda k: stage(far_first(k))
 
     stages = (spread, relay) + tuple(turned(stage) for stage in (compute, first, second))
-    lags = (0, 1, 2 + late, 3 + late, 5 + late)
+    lags = (0, 1, half + 1, half + 2, half + 4)
 
     def step(i, carry):
         for stage, lag in zip(stages, lags):
@@ -795,10 +1061,28 @@
 
     lax.fori_loop(0, n_sp + lags[-1], step, 0)
 
+    def arrive(i, carry):
+        sp_out(i).wait_recv()
+        return carry
+
+    lax.fori_loop(1, n_sp, arrive, 0)
+    share = r.residual.shape[0]
+    width = r.residual.shape[1]
+    tile = math.gcd(width, 512)
+    for n in range(0, width, tile):
+        at = slice(n, n + tile)
+        both = jnp.dot(
+            r.spread[...],
+            r.returned[:, :, :, at].reshape(n_sp * experts * cap, tile),
+            preferred_element_type=jnp.float32,
+        )
+        r.out_ref[:, at] = (
+            r.hidden[:, at].astype(jnp.float32) + (both[:share] + both[share:])
+        ).astype(jnp.bfloat16)
+
     def drain(i, carry):
         @pl.when(i > 0)
         def _():
-            sp_out(i).wait_recv()
             sp_out(i).wait_send()
             sp_copy(i).wait_send()
 
@@ -806,55 +1090,156 @@
             if g:
                 across_in(i, g, mt).wait_send()
                 across_out(i, g).wait_send()
-            if inner == 2:
-                core_in(i, g, mt).wait_send()
-                core_out(i, g).wait_send()
+            core_in(i, g, mt).wait_send()
+            core_out(i, g).wait_send()
         return carry
 
     lax.fori_loop(0, n_sp, drain, 0)
 
 
-def run_experts(n_sp, n_tp, rows, gate_weight, up_weight, down_weight):
-    _, experts, cap, width = rows.shape
-    groups = n_tp // pair_of(n_tp)
+def layer_kernel(n_sp, n_tp, names, *refs):
+    r = types.SimpleNamespace(**dict(zip(names, refs)))
+    me, mt = lax.axis_index("sp"), lax.axis_index("tp")
+    inner = 2
+    z, x = me // inner, me % inner
+    barrier = pltpu.get_barrier_semaphore()
+    lines = [(zz * inner + x, t) for zz in range(n_sp // inner) for t in range(n_tp)]
+    lines += [(zz * inner + (1 - x), mt) for zz in range(n_sp // inner)]
+    for sp, tp in lines:
+
+        @pl.when((sp != me) | (tp != mt))
+        def _():
+            pl.semaphore_signal(
+                barrier, inc=1, device_id={"sp": sp, "tp": tp}, device_id_type=MESH
+            )
+
+    def loads(pairs):
+        copies = [
+            pltpu.make_async_copy(getattr(r, src), getattr(r, dst), r.load_sem.at[k])
+            for k, (src, dst) in pairs
+        ]
+        for copy in copies:
+            copy.start()
+        return copies
+
+    pairs = list(enumerate(LOADED))
+    first = loads(pairs[:5])
+    middle = loads(pairs[5:7])
+    last = loads(pairs[7:])
+    for copy in first:
+        copy.wait()
+
+    def wait_middle():
+        for copy in middle:
+            copy.wait()
+
+    experts, cap = r.outgoing.shape[1:3]
+    attention_phase(
+        n_sp,
+        n_tp,
+        r,
+        lambda: pl.semaphore_wait(barrier, len(lines) - 1),
+        lambda: routing_tables(r, n_sp * experts, cap),
+    )
+    token_phase(r, wait_middle)
+    expert_phase(n_sp, n_tp, r, last)
+
+
+LOADED = (
+    ("k1_hbm", "k1_ref"),
+    ("k2_hbm", "k2_ref"),
+    ("v_hbm", "v_ref"),
+    ("q1_hbm", "q1_ref"),
+    ("q2_hbm", "q2_ref"),
+    ("out_w_hbm", "out_w"),
+    ("residual_hbm", "residual"),
+    ("gate_hbm", "gate_w"),
+    ("up_hbm", "up_w"),
+    ("down_hbm", "down_w"),
+)
+
+
+def whole_layer(n_sp, n_tp, cap, big, lam, gain, norm, ids, logits, prob):
+    k1, k2, v, q1, q2, out_w, residual, gate, up, down = big
+    rows, keys = q1.shape
+    length = n_sp // 2
+    vd = v.shape[1] // 2
+    cols = keys + vd
+    share, width = residual.shape
+    experts = gate.shape[0]
+    slots = n_sp * experts * cap
+    groups = n_tp // 2
+    bf16, f32 = jnp.bfloat16, jnp.float32
+    vmem = pl.BlockSpec(memory_space=pltpu.VMEM)
     dma = pltpu.SemaphoreType.DMA
-    vmem = pl.BlockSpec(memory_space=pltpu.VMEM)
-    hbm = pl.BlockSpec(memory_space=pl.ANY)
     piece = (experts, cap, width)
+    scratch = [(dst, pltpu.VMEM(a.shape, a.dtype)) for (_, dst), a in zip(LOADED, big)]
+    scratch += [
+        ("token_ref", pltpu.VMEM((share, out_w.shape[0]), bf16)),
+        ("kv_out", pltpu.VMEM((2, rows, cols), bf16)),
+        ("q_out", pltpu.VMEM((2, rows, keys), bf16)),
+        ("held", pltpu.VMEM((length, 2, rows, cols), bf16)),
+        ("q_in", pltpu.VMEM((2, rows, keys), bf16)),
+        ("qt", pltpu.VMEM((keys, 4 * rows), bf16)),
+        ("m_ref", pltpu.VMEM((1, 4 * rows), f32)),
+        ("l_ref", pltpu.VMEM((1, 4 * rows), f32)),
+        ("acc_ref", pltpu.VMEM((vd, 4 * rows), f32)),
+        ("stage", pltpu.VMEM((2, rows, vd), bf16)),
+        ("lam_mine", pltpu.VMEM((8, 128), f32)),
+        ("lam_far", pltpu.VMEM((8, 128), f32)),
+        ("table", pltpu.VMEM((slots, share), bf16)),
+        ("spread", pltpu.VMEM((2 * share, slots), bf16)),
+        ("hidden", pltpu.VMEM((share, width), bf16)),
+        ("outgoing", pltpu.VMEM((n_sp,) + piece, bf16)),
+        ("returned", pltpu.VMEM((n_sp,) + piece, bf16)),
+        ("rows", pltpu.VMEM((n_sp, experts, n_tp * cap, width), bf16)),
+        ("part", pltpu.VMEM((n_sp, experts, n_tp * cap, width), bf16)),
+        ("from_core", pltpu.VMEM((n_sp, groups) + piece, bf16)),
+        ("from_across", pltpu.VMEM((n_sp, groups) + piece, bf16)),
+        ("summed", pltpu.VMEM((n_sp, groups) + piece, bf16)),
+        ("total", pltpu.VMEM((n_sp,) + piece, bf16)),
+        ("load_sem", dma((len(LOADED),))),
+        ("first_send", dma((2, 2))),
+        ("core_send", dma((length, 2))),
+        ("side_send", dma((length,))),
+        ("kv_recv", dma((length, 2))),
+        ("q_recv", dma((2,))),
+        ("lam_sem", dma((2,))),
+        ("head_send", dma((2, n_tp))),
+        ("head_recv", dma((2 * n_tp,))),
+        ("sp_send", dma((n_sp,))),
+        ("sp_recv", dma((n_sp,))),
+        ("y_send", dma((groups, n_sp))),
+        ("y_recv", dma((groups, n_sp))),
+        ("c_send", dma((groups, n_sp))),
+        ("c_recv", dma((groups, n_sp))),
+        ("rc_send", dma((n_sp, groups))),
+        ("rc_recv", dma((n_sp, groups))),
+        ("ry_send", dma((n_sp, groups))),
+        ("ry_recv", dma((n_sp, groups))),
+        ("rs_send", dma((n_sp,))),
+        ("rs_recv", dma((n_sp,))),
+    ]
+    small = ("gain_ref", "norm_ref", "ids_ref", "logits_ref", "prob_ref")
+    names = [src for src, _ in LOADED] + ["lam_ref", *small, "out_ref"]
+    names += [name for name, _ in scratch]
     return pl.pallas_call(
-        functools.partial(experts_kernel, n_sp, n_tp),
-        out_shape=jax.ShapeDtypeStruct(rows.shape, rows.dtype),
-        in_specs=[vmem, hbm, hbm, hbm],
+        functools.partial(layer_kernel, n_sp, n_tp, names),
+        out_shape=jax.ShapeDtypeStruct((share, width), bf16),
+        in_specs=[pl.BlockSpec(memory_space=pl.ANY)] * len(LOADED)
+        + [pl.BlockSpec(memory_space=pltpu.SMEM)]
+        + [vmem] * len(small),
         out_specs=vmem,
-        scratch_shapes=[
-            pltpu.VMEM((n_sp, experts, n_tp * cap, width), rows.dtype),
-            pltpu.VMEM((n_sp, experts, n_tp * cap, width), rows.dtype),
-            pltpu.VMEM((n_sp, groups) + piece, rows.dtype),
-            pltpu.VMEM((n_sp, groups) + piece, rows.dtype),
-            pltpu.VMEM((n_sp, groups) + piece, rows.dtype),
-            pltpu.VMEM((n_sp,) + piece, rows.dtype),
-            pltpu.VMEM(gate_weight.shape, gate_weight.dtype),
-            pltpu.VMEM(up_weight.shape, up_weight.dtype),
-            pltpu.VMEM(down_weight.shape, down_weight.dtype),
-            dma((3,)),
-            dma,
-            dma((n_sp,)),
-            dma((n_sp,)),
-            dma((groups, n_sp)),
-            dma((groups, n_sp)),
-            dma((groups, n_sp)),
-            dma((groups, n_sp)),
-            dma((n_sp, groups)),
-            dma((n_sp, groups)),
-            dma((n_sp, groups)),
-            dma((n_sp, groups)),
-            dma((n_sp,)),
-            dma((n_sp,)),
-        ],
+        scratch_shapes=[shape for _, shape in scratch],
         compiler_params=pltpu.CompilerParams(
             collective_id=3, has_side_effects=True, vmem_limit_bytes=VMEM_LIMIT
         ),
-    )(rows, gate_weight, up_weight, down_weight)
+    )(*big, lam, gain, norm, ids, logits, prob)
+
+
+def layers_fit(n_sp, n_tp, rows, vd, keys, heads, cap):
+    square = heads == 2 and n_sp == 8 and n_tp == 4
+    return square and rows % vd == 0 and vd == keys and vd % 128 == 0 and cap % 16 == 0
 
 
 def on_device(
@@ -877,6 +1262,33 @@
     up_weight,
     down_weight,
 ):
+    share = residual_in.shape[0]
+    top_count = route_ids.shape[1]
+    local_experts = gate_weight.shape[0]
+    expert_count = local_experts * n_sp
+    capacity = max(2, 2 * share * top_count // expert_count)
+    if layers_fit(
+        n_sp,
+        n_tp,
+        query_one.shape[0],
+        values.shape[1] // 2,
+        query_one.shape[1],
+        mix_lambda.shape[0],
+        capacity,
+    ):
+        big = (key_one, key_two, values, query_one, query_two, out_weight, residual_in)
+        return whole_layer(
+            n_sp,
+            n_tp,
+            capacity,
+            big + (gate_weight, up_weight, down_weight),
+            mix_lambda,
+            head_gain[None, :],
+            norm_gain[None, :],
+            route_ids.T,
+            route_logits.T,
+            group_prob[None, :],
+        )
     token_heads = attend(
         n_sp,
         n_tp,
@@ -888,7 +1300,6 @@
         mix_lambda,
         head_gain[None, :],
     )
-    share = residual_in.shape[0]
     mix = jnp.dot(token_heads, out_weight, preferred_element_type=jnp.float32)
     hidden_f = (residual_in.astype(jnp.float32) + mix).astype(jnp.bfloat16).astype(jnp.float32)
     normed = (
@@ -897,10 +1308,6 @@
         * norm_gain
     ).astype(jnp.bfloat16)
     width = normed.shape[1]
-    top_count = route_ids.shape[1]
-    local_experts = gate_weight.shape[0]
-    expert_count = local_experts * n_sp
-    capacity = max(2, 2 * share * top_count // expert_count)
     slots = expert_count * capacity
     flat_ids = route_ids.reshape(-1)
     one_hot = (flat_ids[:, None] == jnp.arange(expert_count, dtype=jnp.int32)[None, :]).astype(
@@ -915,23 +1322,18 @@
     )
     outgoing = jnp.dot(table, normed, preferred_element_type=jnp.float32).astype(jnp.bfloat16)
     outgoing = outgoing.reshape(n_sp, local_experts, capacity, width)
-    if capacity % 16 == 0:
-        returned = run_experts(
-            n_sp, n_tp, outgoing, gate_weight, up_weight, down_weight
-        ).reshape(slots, width)
-    else:
-        everyone = dispatch(
-            n_sp, n_tp, outgoing
-        ).reshape(local_experts, n_tp * n_sp * capacity, width)
-        gate = jnp.einsum("erd,edf->erf", everyone, gate_weight, preferred_element_type=jnp.float32)
-        upper = jnp.einsum("erd,edf->erf", everyone, up_weight, preferred_element_type=jnp.float32)
-        middle = (jax.nn.silu(gate) * upper).astype(jnp.bfloat16)
-        part_sum = jnp.einsum(
-            "erf,efd->erd", middle, down_weight, preferred_element_type=jnp.float32
-        ).astype(jnp.bfloat16)
-        returned = collect(
-            n_sp, n_tp, part_sum.reshape(local_experts, n_tp, n_sp, capacity, width)
-        ).reshape(slots, width)
+    everyone = dispatch(n_sp, n_tp, outgoing).reshape(
+        local_experts, n_tp * n_sp * capacity, width
+    )
+    gate = jnp.einsum("erd,edf->erf", everyone, gate_weight, preferred_element_type=jnp.float32)
+    upper = jnp.einsum("erd,edf->erf", everyone, up_weight, preferred_element_type=jnp.float32)
+    middle = (jax.nn.silu(gate) * upper).astype(jnp.bfloat16)
+    part_sum = jnp.einsum(
+        "erf,efd->erd", middle, down_weight, preferred_element_type=jnp.float32
+    ).astype(jnp.bfloat16)
+    returned = collect(
+        n_sp, n_tp, part_sum.reshape(local_experts, n_tp, n_sp, capacity, width)
+    ).reshape(slots, width)
     logits = [route_logits[:, k : k + 1] for k in range(top_count)]
     highest = functools.reduce(jnp.maximum, logits)
     powers = [jnp.exp(logit - highest) for logit in logits]

time: 113 us -> 98.8 us (0.87)
  matrix products: 6.24 us -> 0 us
  Pallas kernels: 103 us -> 96.9 us
  other arithmetic: 2.79 us -> 0 us
    dot_general x3 -> x0, matrix products: 6.24 us -> none  [the longest x1 3.22 us: on_device(): mix = jnp.dot(token_heads, out_weight, preferred_element_type=jnp.float32)]
    pallas_call x2 -> x1, Pallas kernels: 103 us -> 96.9 us  [whole_layer(): pl.pallas_call(functools.partial(layer_kernel, n_sp, n_tp, names), out_sh...]
where the time goes in v2:
time: 98.8 us; the launch traced here: 98.6 us
  Pallas kernels  96.9 us (98%)
  local copies, waits for them, and re-layouts  1.67 us (2%)
    pallas_call x1, Pallas kernels, whole_layer(): pl.pallas_call(functools.partial(layer_kernel, n_sp, n_tp, names), out_sh...  96.9 us

profile of v2, /device:TPU:0, one launch (start us, length us, event | category | flops | bytes accessed | tf_op | source)
XLA Modules:
  0.0 98.6 jit_solution(8095086809740837391)
XLA Ops:
  0.0 96.9 %shard_map.154 = bf16[64,2048]{1,0:T(8,128)(2,1)} custom-call(bf16[256,128]{1,0:T(8,128)(2,1)} %refs_0_.1, bf16[256,128]{1,0:T(8,128)(2,1)} %refs_1_.1, bf16[256,256]{1,0:T(8,128)(2,1)} %refs_2_.1, bf16[256,128]{1,0:T(8,128)(2,1)} %refs_3_.1, bf16[256,128]{1,0:T(8,128)(2,1)} %refs_4_.1, bf16[1024,2048]{1,0:T(8,128)(2,1)} %refs_5_.1, ...), custom_call_target="tpu_custom_call" | custom-call | tf_op jit(solution)/shard_map/pallas_call | solution.py:1226
  96.9 1.7 %copy.18 = bf16[64,2048]{1,0:T(8,128)(2,1)} copy(bf16[64,2048]{1,0:T(8,128)(2,1)} %shard_map.154) | data formatting | bytes 524288

commit v3 on v2

--- a/solution.py
+++ b/solution.py
@@ -12,6 +12,7 @@
 norm_epsilon = 1e-06
 MESH = pl.DeviceIdType.MESH
 VMEM_LIMIT = 60 * 1024 * 1024
+LAYER_LIMIT = VMEM_LIMIT
 
 
 def pair_of(count):
@@ -935,137 +936,142 @@
             device_id_type=MESH,
         )
 
-    def sp_copy(i):
+    pieces = n_sp * experts
+
+    def sp_copy(j):
+        i, e = j // experts, j % experts
         to = peer_of(i)
-        block = r.rows.at[i, :, span(mt)]
-        return remote(r.outgoing.at[to], block, r.sp_send.at[i], r.sp_recv.at[i], to, mt)
-
-    def across_in(i, g, t):
-        block = r.rows.at[i, :, span(t)]
-        return remote(block, block, r.y_send.at[g, i], r.y_recv.at[g, i], me, across[g - 1])
-
-    def core_in(i, g, t):
-        block = r.rows.at[i, :, span(t)]
-        return remote(block, block, r.c_send.at[g, i], r.c_recv.at[g, i], me, partner)
-
-    def core_out(i, g):
+        block = r.rows.at[i, e, span(mt)]
+        return remote(r.outgoing.at[to, e], block, r.sp_send.at[j], r.sp_recv.at[j], to, mt)
+
+    def across_in(j, g, t):
+        block = r.rows.at[j // experts, j % experts, span(t)]
+        return remote(block, block, r.y_send.at[g, j], r.y_recv.at[g, j], me, across[g - 1])
+
+    def core_in(j, g, t):
+        block = r.rows.at[j // experts, j % experts, span(t)]
+        return remote(block, block, r.c_send.at[g, j], r.c_recv.at[g, j], me, partner)
+
+    def core_out(j, g):
         row = ((o + g) % groups) * inner + (inner - 1 - c)
-        block = r.part.at[i, :, span(row)]
+        block = r.part.at[j, span(row)]
         return remote(
-            block, r.from_core.at[i, g], r.rc_send.at[i, g], r.rc_recv.at[i, g], me, partner
-        )
-
-    def across_out(i, g):
+            block, r.from_core.at[j, g], r.rc_send.at[j, g], r.rc_recv.at[j, g], me, partner
+        )
+
+    def across_out(j, g):
         return remote(
-            r.summed.at[i, g],
-            r.from_across.at[i, g],
-            r.ry_send.at[i, g],
-            r.ry_recv.at[i, g],
+            r.summed.at[j, g],
+            r.from_across.at[j, g],
+            r.ry_send.at[j, g],
+            r.ry_recv.at[j, g],
             me,
             across[g - 1],
         )
 
-    def sp_out(i):
-        return remote(
-            r.total.at[i], r.returned.at[me], r.rs_send.at[i], r.rs_recv.at[i], peer_of(i), mt
-        )
+    def sp_out(j):
+        i, e = j // experts, j % experts
+        block = r.returned.at[me, e]
+        return remote(r.total.at[j], block, r.rs_send.at[j], r.rs_recv.at[j], peer_of(i), mt)
 
     def source(g):
         return ((o - g + groups) % groups) * inner + c
 
-    for i in range(1, n_sp):
-        sp_copy(i).start()
+    for j in range(experts, pieces):
+        sp_copy(j).start()
     r.rows[0, :, span(mt), :] = r.outgoing[me]
 
-    def spread(i):
-        @pl.when(i > 0)
-        def _():
-            sp_copy(i).wait_recv()
+    def spread(j):
+        @pl.when(j >= experts)
+        def _():
+            sp_copy(j).wait_recv()
 
         for g in range(1, groups):
-            across_in(i, g, mt).start()
-        core_in(i, 0, mt).start()
-
-    def relay(i):
+            across_in(j, g, mt).start()
+        core_in(j, 0, mt).start()
+
+    def relay(j):
         for g in range(1, groups):
-            across_in(i, g, source(g)).wait_recv()
-            core_in(i, g, source(g)).start()
+            across_in(j, g, source(g)).wait_recv()
+            core_in(j, g, source(g)).start()
 
     half = n_sp // 2
 
-    def compute(i):
-        @pl.when(i == half)
+    def compute(j):
+        @pl.when(j == half * experts)
         def _():
             for copy in weights:
                 copy.wait()
 
         for g in range(groups):
-            core_in(i, g, source(g)).wait_recv()
-        for e in range(experts):
-            rows = r.rows[i, e]
-            gate = jnp.dot(rows, r.gate_w[e], preferred_element_type=jnp.float32)
-            upper = jnp.dot(rows, r.up_w[e], preferred_element_type=jnp.float32)
-            middle = (gate / (1.0 + jnp.exp(-gate)) * upper).astype(jnp.bfloat16)
-            r.part[i, e] = jnp.dot(middle, r.down_w[e], preferred_element_type=jnp.float32).astype(
-                r.part.dtype
-            )
+            core_in(j, g, source(g)).wait_recv()
+        e = j % experts
+        rows = r.rows[j // experts, e]
+        gate = jnp.dot(rows, r.gate_w[e], preferred_element_type=jnp.float32)
+        upper = jnp.dot(rows, r.up_w[e], preferred_element_type=jnp.float32)
+        middle = (gate / (1.0 + jnp.exp(-gate)) * upper).astype(jnp.bfloat16)
+        r.part[j] = jnp.dot(middle, r.down_w[e], preferred_element_type=jnp.float32).astype(
+            r.part.dtype
+        )
         for g in list(range(1, groups)) + [0]:
-            core_out(i, g).start()
-
-    def pair_sum(i, g):
+            core_out(j, g).start()
+
+    def pair_sum(j, g):
         row = ((o + g) % groups) * inner + c
-        value = r.part[i, :, span(row), :].astype(jnp.float32)
-        core_out(i, g).wait_recv()
-        return value + r.from_core[i, g].astype(jnp.float32)
-
-    def first(i):
+        value = r.part[j, span(row), :].astype(jnp.float32)
+        core_out(j, g).wait_recv()
+        return value + r.from_core[j, g].astype(jnp.float32)
+
+    def first(j):
         for g in range(1, groups):
-            r.summed[i, g] = pair_sum(i, g).astype(r.summed.dtype)
-            across_out(i, g).start()
-
-    def second(i):
-        value = pair_sum(i, 0)
+            r.summed[j, g] = pair_sum(j, g).astype(r.summed.dtype)
+            across_out(j, g).start()
+
+    def second(j):
+        value = pair_sum(j, 0)
         for g in range(1, groups):
-            across_out(i, g).wait_recv()
-            value = value + r.from_across[i, g].astype(jnp.float32)
+            across_out(j, g).wait_recv()
+            value = value + r.from_across[j, g].astype(jnp.float32)
         value = value.astype(r.total.dtype)
 
-        @pl.when(i == 0)
-        def _():
-            r.returned[me] = value
-
-        @pl.when(i > 0)
-        def _():
-            r.total[i] = value
-            sp_out(i).start()
-
-    def far_first(k):
+        @pl.when(j < experts)
+        def _():
+            r.returned[me, j] = value
+
+        @pl.when(j >= experts)
+        def _():
+            r.total[j] = value
+            sp_out(j).start()
+
+    def far_first(n):
+        k, e = n // experts, n % experts
         near = n_sp - 1 - k
         near = jnp.where(near > 1, half // 2 + n_sp - 1 - half - near, near)
-        return jnp.where(k < half, k + half, near)
+        return jnp.where(k < half, k + half, near) * experts + e
 
     def turned(stage):
-        return lambda k: stage(far_first(k))
+        return lambda n: stage(far_first(n))
 
     stages = (spread, relay) + tuple(turned(stage) for stage in (compute, first, second))
-    lags = (0, 1, half + 1, half + 2, half + 4)
-
-    def step(i, carry):
+    ready = half * experts
+    lags = (0, 3, ready + 4, ready + 6, ready + 9)
+
+    def step(n, carry):
         for stage, lag in zip(stages, lags):
 
-            @pl.when((i >= lag) & (i < n_sp + lag))
+            @pl.when((n >= lag) & (n < pieces + lag))
             def _():
-                stage(i - lag)
+                stage(n - lag)
 
         return carry
 
-    lax.fori_loop(0, n_sp + lags[-1], step, 0)
-
-    def arrive(i, carry):
-        sp_out(i).wait_recv()
+    lax.fori_loop(0, pieces + lags[-1], step, 0)
+
+    def arrive(j, carry):
+        sp_out(j).wait_recv()
         return carry
 
-    lax.fori_loop(1, n_sp, arrive, 0)
+    lax.fori_loop(experts, pieces, arrive, 0)
     share = r.residual.shape[0]
     width = r.residual.shape[1]
     tile = math.gcd(width, 512)
@@ -1073,28 +1079,26 @@
         at = slice(n, n + tile)
         both = jnp.dot(
             r.spread[...],
-            r.returned[:, :, :, at].reshape(n_sp * experts * cap, tile),
+            r.returned[:, :, :, at].reshape(pieces * cap, tile),
             preferred_element_type=jnp.float32,
         )
-        r.out_ref[:, at] = (
-            r.hidden[:, at].astype(jnp.float32) + (both[:share] + both[share:])
-        ).astype(jnp.bfloat16)
-
-    def drain(i, carry):
-        @pl.when(i > 0)
-        def _():
-            sp_out(i).wait_send()
-            sp_copy(i).wait_send()
+        r.out_ref[:, at] = (r.hidden[:, at].astype(jnp.float32) + (both[:share] + both[share:])).astype(jnp.bfloat16)
+
+    def drain(j, carry):
+        @pl.when(j >= experts)
+        def _():
+            sp_out(j).wait_send()
+            sp_copy(j).wait_send()
 
         for g in range(groups):
             if g:
-                across_in(i, g, mt).wait_send()
-                across_out(i, g).wait_send()
-            core_in(i, g, mt).wait_send()
-            core_out(i, g).wait_send()
+                across_in(j, g, mt).wait_send()
+                across_out(j, g).wait_send()
+            core_in(j, g, mt).wait_send()
+            core_out(j, g).wait_send()
         return carry
 
-    lax.fori_loop(0, n_sp, drain, 0)
+    lax.fori_loop(0, pieces, drain, 0)
 
 
 def layer_kernel(n_sp, n_tp, names, *refs):
@@ -1167,7 +1171,8 @@
     cols = keys + vd
     share, width = residual.shape
     experts = gate.shape[0]
-    slots = n_sp * experts * cap
+    pieces = n_sp * experts
+    slots = pieces * cap
     groups = n_tp // 2
     bf16, f32 = jnp.bfloat16, jnp.float32
     vmem = pl.BlockSpec(memory_space=pltpu.VMEM)
@@ -1193,11 +1198,11 @@
         ("outgoing", pltpu.VMEM((n_sp,) + piece, bf16)),
         ("returned", pltpu.VMEM((n_sp,) + piece, bf16)),
         ("rows", pltpu.VMEM((n_sp, experts, n_tp * cap, width), bf16)),
-        ("part", pltpu.VMEM((n_sp, experts, n_tp * cap, width), bf16)),
-        ("from_core", pltpu.VMEM((n_sp, groups) + piece, bf16)),
-        ("from_across", pltpu.VMEM((n_sp, groups) + piece, bf16)),
-        ("summed", pltpu.VMEM((n_sp, groups) + piece, bf16)),
-        ("total", pltpu.VMEM((n_sp,) + piece, bf16)),
+        ("part", pltpu.VMEM((pieces, n_tp * cap, width), bf16)),
+        ("from_core", pltpu.VMEM((pieces, groups, cap, width), bf16)),
+        ("from_across", pltpu.VMEM((pieces, groups, cap, width), bf16)),
+        ("summed", pltpu.VMEM((pieces, groups, cap, width), bf16)),
+        ("total", pltpu.VMEM((pieces, cap, width), bf16)),
         ("load_sem", dma((len(LOADED),))),
         ("first_send", dma((2, 2))),
         ("core_send", dma((length, 2))),
@@ -1207,18 +1212,18 @@
         ("lam_sem", dma((2,))),
         ("head_send", dma((2, n_tp))),
         ("head_recv", dma((2 * n_tp,))),
-        ("sp_send", dma((n_sp,))),
-        ("sp_recv", dma((n_sp,))),
-        ("y_send", dma((groups, n_sp))),
-        ("y_recv", dma((groups, n_sp))),
-        ("c_send", dma((groups, n_sp))),
-        ("c_recv", dma((groups, n_sp))),
-        ("rc_send", dma((n_sp, groups))),
-        ("rc_recv", dma((n_sp, groups))),
-        ("ry_send", dma((n_sp, groups))),
-        ("ry_recv", dma((n_sp, groups))),
-        ("rs_send", dma((n_sp,))),
-        ("rs_recv", dma((n_sp,))),
+        ("sp_send", dma((pieces,))),
+        ("sp_recv", dma((pieces,))),
+        ("y_send", dma((groups, pieces))),
+        ("y_recv", dma((groups, pieces))),
+        ("c_send", dma((groups, pieces))),
+        ("c_recv", dma((groups, pieces))),
+        ("rc_send", dma((pieces, groups))),
+        ("rc_recv", dma((pieces, groups))),
+        ("ry_send", dma((pieces, groups))),
+        ("ry_recv", dma((pieces, groups))),
+        ("rs_send", dma((pieces,))),
+        ("rs_recv", dma((pieces,))),
     ]
     small = ("gain_ref", "norm_ref", "ids_ref", "logits_ref", "prob_ref")
     names = [src for src, _ in LOADED] + ["lam_ref", *small, "out_ref"]
@@ -1226,13 +1231,13 @@
     return pl.pallas_call(
         functools.partial(layer_kernel, n_sp, n_tp, names),
         out_shape=jax.ShapeDtypeStruct((share, width), bf16),
-        in_specs=[pl.BlockSpec(memory_space=pl.ANY)] * len(LOADED)
+        in_specs=[pl.BlockSpec(memory_space=pltpu.HBM)] * len(LOADED)
         + [pl.BlockSpec(memory_space=pltpu.SMEM)]
         + [vmem] * len(small),
         out_specs=vmem,
         scratch_shapes=[shape for _, shape in scratch],
         compiler_params=pltpu.CompilerParams(
-            collective_id=3, has_side_effects=True, vmem_limit_bytes=VMEM_LIMIT
+            collective_id=3, has_side_effects=True, vmem_limit_bytes=LAYER_LIMIT
         ),
     )(*big, lam, gain, norm, ids, logits, prob)
 

time: 98.8 us -> 92.2 us (0.933)
  Pallas kernels: 96.9 us -> 90.4 us
    pallas_call x1, Pallas kernels: 96.9 us -> 90.4 us  [whole_layer(): pl.pallas_call(functools.partial(layer_kernel, n_sp, n_tp, names), out_sh...]
where the time goes in v3:
time: 92.2 us; the launch traced here: 92.1 us
  Pallas kernels  90.4 us (98%)
  local copies, waits for them, and re-layouts  1.67 us (2%)
    pallas_call x1, Pallas kernels, whole_layer(): pl.pallas_call(functools.partial(layer_kernel, n_sp, n_tp, names), out_sh...  90.4 us

profile of v3, /device:TPU:0, one launch (start us, length us, event | category | flops | bytes accessed | tf_op | source)
XLA Modules:
  0.0 92.1 jit_solution(963172926309586898)
XLA Ops:
  0.0 90.4 %shard_map.154 = bf16[64,2048]{1,0:T(8,128)(2,1)} custom-call(bf16[256,128]{1,0:T(8,128)(2,1)} %refs_0_.1, bf16[256,128]{1,0:T(8,128)(2,1)} %refs_1_.1, bf16[256,256]{1,0:T(8,128)(2,1)} %refs_2_.1, bf16[256,128]{1,0:T(8,128)(2,1)} %refs_3_.1, bf16[256,128]{1,0:T(8,128)(2,1)} %refs_4_.1, bf16[1024,2048]{1,0:T(8,128)(2,1)} %refs_5_.1, ...), custom_call_target="tpu_custom_call" | custom-call | tf_op jit(solution)/shard_map/pallas_call | solution.py:1231
  90.4 1.7 %copy.18 = bf16[64,2048]{1,0:T(8,128)(2,1)} copy(bf16[64,2048]{1,0:T(8,128)(2,1)} %shard_map.154) | data formatting | bytes 524288

commit v4 on v3

--- a/solution.py
+++ b/solution.py
@@ -833,26 +833,29 @@
         def _():
             head_copy(hd).wait_recv()
 
-    for g in range(2):
-        for t in range(1, n_tp):
-            piece(g, t).wait_send()
-
-        @pl.when(jnp.logical_not(own(g)))
-        def _():
-            piece(g, 0).wait_send()
-
-        @pl.when(away(g))
-        def _():
-            first_q(g).wait_send()
-            first_kv(g).wait_send()
-
-    for zz in range(length):
-
-        @pl.when(c == zz // pair)
-        def _():
-            to_side(zz).wait_send()
-            to_core(zz, 0).wait_send()
-            to_core(zz, 1).wait_send()
+    def finish():
+        for g in range(2):
+            for t in range(1, n_tp):
+                piece(g, t).wait_send()
+
+            @pl.when(jnp.logical_not(own(g)))
+            def _():
+                piece(g, 0).wait_send()
+
+            @pl.when(away(g))
+            def _():
+                first_q(g).wait_send()
+                first_kv(g).wait_send()
+
+        for zz in range(length):
+
+            @pl.when(c == zz // pair)
+            def _():
+                to_side(zz).wait_send()
+                to_core(zz, 0).wait_send()
+                to_core(zz, 1).wait_send()
+
+    return finish
 
 
 def routing_tables(r, experts_in_all, cap):
@@ -907,7 +910,7 @@
         r.outgoing[:, :, :, at] = rows.reshape(n_sp, experts, cap, tile)
 
 
-def expert_phase(n_sp, n_tp, r, weights):
+def expert_phase(n_sp, n_tp, r, weights, finish):
     me, mt = lax.axis_index("sp"), lax.axis_index("tp")
     inner_sp = 2
     z, x = me // inner_sp, me % inner_sp
@@ -977,7 +980,7 @@
     def source(g):
         return ((o - g + groups) % groups) * inner + c
 
-    for j in range(experts, pieces):
+    for j in (2, 8, 4, 3, 9, 5, 10, 6, 11, 7, 12, 13, 14, 15):
         sp_copy(j).start()
     r.rows[0, :, span(mt), :] = r.outgoing[me]
 
@@ -996,9 +999,10 @@
             core_in(j, g, source(g)).start()
 
     half = n_sp // 2
+    ready = half * experts
 
     def compute(j):
-        @pl.when(j == half * experts)
+        @pl.when(j == ready)
         def _():
             for copy in weights:
                 copy.wait()
@@ -1044,17 +1048,18 @@
             sp_out(j).start()
 
     def far_first(n):
-        k, e = n // experts, n % experts
-        near = n_sp - 1 - k
-        near = jnp.where(near > 1, half // 2 + n_sp - 1 - half - near, near)
-        return jnp.where(k < half, k + half, near) * experts + e
+        near = jnp.where(n < ready + half, n - half, jnp.where(n < ready + 6, n - 10, n - 14))
+        return jnp.where(n < ready, n + ready, near)
+
+    def arrival(n):
+        mixed = n // 2 + jnp.where(n % 2 == 0, 6, 2)
+        return jnp.where((n < half) | (n >= ready + half), n, mixed)
 
     def turned(stage):
         return lambda n: stage(far_first(n))
 
-    stages = (spread, relay) + tuple(turned(stage) for stage in (compute, first, second))
-    ready = half * experts
-    lags = (0, 3, ready + 4, ready + 6, ready + 9)
+    stages = tuple((lambda n, f=f: f(arrival(n))) for f in (spread, relay)) + tuple(turned(stage) for stage in (compute, first, second))
+    lags = (0, 3, 12, 14, 17)
 
     def step(n, carry):
         for stage, lag in zip(stages, lags):
@@ -1066,6 +1071,24 @@
         return carry
 
     lax.fori_loop(0, pieces + lags[-1], step, 0)
+
+    finish()
+
+    def drain(j, carry):
+        @pl.when(j >= experts)
+        def _():
+            sp_out(j).wait_send()
+            sp_copy(j).wait_send()
+
+        for g in range(groups):
+            if g:
+                across_in(j, g, mt).wait_send()
+                across_out(j, g).wait_send()
+            core_in(j, g, mt).wait_send()
+            core_out(j, g).wait_send()
+        return carry
+
+    lax.fori_loop(0, pieces, drain, 0)
 
     def arrive(j, carry):
         sp_out(j).wait_recv()
@@ -1084,22 +1107,6 @@
         )
         r.out_ref[:, at] = (r.hidden[:, at].astype(jnp.float32) + (both[:share] + both[share:])).astype(jnp.bfloat16)
 
-    def drain(j, carry):
-        @pl.when(j >= experts)
-        def _():
-            sp_out(j).wait_send()
-            sp_copy(j).wait_send()
-
-        for g in range(groups):
-            if g:
-                across_in(j, g, mt).wait_send()
-                across_out(j, g).wait_send()
-            core_in(j, g, mt).wait_send()
-            core_out(j, g).wait_send()
-        return carry
-
-    lax.fori_loop(0, pieces, drain, 0)
-
 
 def layer_kernel(n_sp, n_tp, names, *refs):
     r = types.SimpleNamespace(**dict(zip(names, refs)))
@@ -1138,7 +1145,7 @@
             copy.wait()
 
     experts, cap = r.outgoing.shape[1:3]
-    attention_phase(
+    finish = attention_phase(
         n_sp,
         n_tp,
         r,
@@ -1146,7 +1153,7 @@
         lambda: routing_tables(r, n_sp * experts, cap),
     )
     token_phase(r, wait_middle)
-    expert_phase(n_sp, n_tp, r, last)
+    expert_phase(n_sp, n_tp, r, last, finish)
 
 
 LOADED = (
@@ -1242,8 +1249,8 @@
     )(*big, lam, gain, norm, ids, logits, prob)
 
 
-def layers_fit(n_sp, n_tp, rows, vd, keys, heads, cap):
-    square = heads == 2 and n_sp == 8 and n_tp == 4
+def layers_fit(n_sp, n_tp, rows, vd, keys, heads, experts, cap):
+    square = heads == 2 and experts == 2 and n_sp == 8 and n_tp == 4
     return square and rows % vd == 0 and vd == keys and vd % 128 == 0 and cap % 16 == 0
 
 
@@ -1279,6 +1286,7 @@
         values.shape[1] // 2,
         query_one.shape[1],
         mix_lambda.shape[0],
+        local_experts,
         capacity,
     ):
         big = (key_one, key_two, values, query_one, query_two, out_weight, residual_in)

time: 92.2 us -> 90.3 us (0.979)
  Pallas kernels: 90.4 us -> 88.4 us
    pallas_call x1, Pallas kernels: 90.4 us -> 88.4 us  [whole_layer(): pl.pallas_call(functools.partial(layer_kernel, n_sp, n_tp, names), out_sh...]
where the time goes in v4:
time: 90.3 us; the launch traced here: 90.1 us
  Pallas kernels  88.4 us (98%)
  local copies, waits for them, and re-layouts  1.67 us (2%)
    pallas_call x1, Pallas kernels, whole_layer(): pl.pallas_call(functools.partial(layer_kernel, n_sp, n_tp, names), out_sh...  88.4 us

profile of v4, /device:TPU:0, one launch (start us, length us, event | category | flops | bytes accessed | tf_op | source)
XLA Modules:
  0.0 90.1 jit_solution(12885525921055099966)
XLA Ops:
  0.0 88.4 %shard_map.154 = bf16[64,2048]{1,0:T(8,128)(2,1)} custom-call(bf16[256,128]{1,0:T(8,128)(2,1)} %refs_0_.1, bf16[256,128]{1,0:T(8,128)(2,1)} %refs_1_.1, bf16[256,256]{1,0:T(8,128)(2,1)} %refs_2_.1, bf16[256,128]{1,0:T(8,128)(2,1)} %refs_3_.1, bf16[256,128]{1,0:T(8,128)(2,1)} %refs_4_.1, bf16[1024,2048]{1,0:T(8,128)(2,1)} %refs_5_.1, ...), custom_call_target="tpu_custom_call" | custom-call | tf_op jit(solution)/shard_map/pallas_call | solution.py:1238
  88.4 1.7 %copy.18 = bf16[64,2048]{1,0:T(8,128)(2,1)} copy(bf16[64,2048]{1,0:T(8,128)(2,1)} %shard_map.154) | data formatting | bytes 524288

commit v5 on v4

--- a/solution.py
+++ b/solution.py
@@ -1052,7 +1052,7 @@
         return jnp.where(n < ready, n + ready, near)
 
     def arrival(n):
-        mixed = n // 2 + jnp.where(n % 2 == 0, 6, 2)
+        mixed = n // 2 + jnp.where(n % 2 == 0, 2, 6)
         return jnp.where((n < half) | (n >= ready + half), n, mixed)
 
     def turned(stage):
@@ -1237,7 +1237,7 @@
     names += [name for name, _ in scratch]
     return pl.pallas_call(
         functools.partial(layer_kernel, n_sp, n_tp, names),
-        out_shape=jax.ShapeDtypeStruct((share, width), bf16),
+        out_shape=pltpu.VMEM((share, width), bf16),
         in_specs=[pl.BlockSpec(memory_space=pltpu.HBM)] * len(LOADED)
         + [pl.BlockSpec(memory_space=pltpu.SMEM)]
         + [vmem] * len(small),

time: 90.3 us -> 88.4 us (0.979)
  local copies, waits for them, and re-layouts: 1.67 us -> 0.71 us
    unnamed x1, local copies, waits for them, and re-layouts: 1.67 us -> 0.71 us
    pallas_call x1, Pallas kernels: 88.4 us -> 87.5 us  [whole_layer(): pl.pallas_call(functools.partial(layer_kernel, n_sp, n_tp, names), out_sh...]
where the time goes in v5:
time: 88.4 us; the launch traced here: 88.2 us
  Pallas kernels  87.5 us (99%)
    pallas_call x1, Pallas kernels, whole_layer(): pl.pallas_call(functools.partial(layer_kernel, n_sp, n_tp, names), out_sh...  87.5 us

profile of v5, /device:TPU:0, one launch (start us, length us, event | category | flops | bytes accessed | tf_op | source)
XLA Modules:
  0.0 88.2 jit_solution(13369617622691349552)
XLA Ops:
  0.0 87.5 %shard_map.154 = bf16[64,2048]{1,0:T(8,128)(2,1)S(1)} custom-call(bf16[256,128]{1,0:T(8,128)(2,1)} %refs_0_.1, bf16[256,128]{1,0:T(8,128)(2,1)} %refs_1_.1, bf16[256,256]{1,0:T(8,128)(2,1)} %refs_2_.1, bf16[256,128]{1,0:T(8,128)(2,1)} %refs_3_.1, bf16[256,128]{1,0:T(8,128)(2,1)} %refs_4_.1, bf16[1024,2048]{1,0:T(8,128)(2,1)} %refs_5_.1, ...), custom_call_target="tpu_custom_call" | custom-call | tf_op jit(solution)/shard_map/pallas_call | solution.py:1238
  87.5 0.7 copy.18

commit v6 on v5

--- a/solution.py
+++ b/solution.py
@@ -827,11 +827,13 @@
             r.stage.at[0, 0:share], r.token_ref.at[:, at], r.head_send.at[0, 0], r.head_recv.at[hd], me, mt
         )
 
-    for hd in range(2 * n_tp):
-
-        @pl.when((hd != head) | jnp.logical_not(home))
-        def _():
-            head_copy(hd).wait_recv()
+    def heads_of(plane):
+        for k in range(length):
+            hd = plane * length + k
+
+            @pl.when((hd != head) | jnp.logical_not(home))
+            def _():
+                head_copy(hd).wait_recv()
 
     def finish():
         for g in range(2):
@@ -855,7 +857,7 @@
                 to_core(zz, 0).wait_send()
                 to_core(zz, 1).wait_send()
 
-    return finish
+    return finish, heads_of
 
 
 def routing_tables(r, experts_in_all, cap):
@@ -888,15 +890,26 @@
     r.spread[share : 2 * share] = (turned - high.astype(jnp.float32)).astype(jnp.bfloat16)
 
 
-def token_phase(r, wait_weights):
+def token_phase(r, wait_weights, y, heads_of):
     share, width = r.residual.shape
     tile = math.gcd(width, 512)
     columns = [slice(n, n + tile) for n in range(0, width, tile)]
     wait_weights()
+    depth = r.token_ref.shape[1] // 2
+
+    def plane_mix(plane, at):
+        span = pl.ds(pl.multiple_of(plane * depth, depth), depth)
+        return jnp.dot(
+            r.token_ref[:, span], r.out_w[span, at], preferred_element_type=jnp.float32
+        )
+
+    heads_of(y)
+    for at in columns:
+        r.mix[:, at] = plane_mix(y, at) + r.residual[:, at].astype(jnp.float32)
+    heads_of(1 - y)
     square = jnp.zeros((share, 1), jnp.float32)
     for at in columns:
-        mix = jnp.dot(r.token_ref[...], r.out_w[:, at], preferred_element_type=jnp.float32)
-        hidden = (r.residual[:, at].astype(jnp.float32) + mix).astype(jnp.bfloat16)
+        hidden = (r.mix[:, at] + plane_mix(1 - y, at)).astype(jnp.bfloat16)
         r.hidden[:, at] = hidden
         hidden = hidden.astype(jnp.float32)
         square = square + jnp.sum(hidden * hidden, axis=1, keepdims=True)
@@ -1145,14 +1158,14 @@
             copy.wait()
 
     experts, cap = r.outgoing.shape[1:3]
-    finish = attention_phase(
+    finish, heads_of = attention_phase(
         n_sp,
         n_tp,
         r,
         lambda: pl.semaphore_wait(barrier, len(lines) - 1),
         lambda: routing_tables(r, n_sp * experts, cap),
     )
-    token_phase(r, wait_middle)
+    token_phase(r, wait_middle, mt // 2, heads_of)
     expert_phase(n_sp, n_tp, r, last, finish)
 
 
@@ -1201,6 +1214,7 @@
         ("lam_far", pltpu.VMEM((8, 128), f32)),
         ("table", pltpu.VMEM((slots, share), bf16)),
         ("spread", pltpu.VMEM((2 * share, slots), bf16)),
+        ("mix", pltpu.VMEM((share, width), f32)),
         ("hidden", pltpu.VMEM((share, width), bf16)),
         ("outgoing", pltpu.VMEM((n_sp,) + piece, bf16)),
         ("returned", pltpu.VMEM((n_sp,) + piece, bf16)),

time: 88.4 us -> 88.4 us (level)
  no operation moved by 1% of the time
where the time goes in v6:
time: 88.4 us; the launch traced here: 88.2 us
  Pallas kernels  87.5 us (99%)
    pallas_call x1, Pallas kernels, whole_layer(): pl.pallas_call(functools.partial(layer_kernel, n_sp, n_tp, names), out_sh...  87.5 us

profile of v6, /device:TPU:0, one launch (start us, length us, event | category | flops | bytes accessed | tf_op | source)
XLA Modules:
  0.0 88.2 jit_solution(4394188507395936172)
XLA Ops:
  0.0 87.5 %shard_map.154 = bf16[64,2048]{1,0:T(8,128)(2,1)S(1)} custom-call(bf16[256,128]{1,0:T(8,128)(2,1)} %refs_0_.1, bf16[256,128]{1,0:T(8,128)(2,1)} %refs_1_.1, bf16[256,256]{1,0:T(8,128)(2,1)} %refs_2_.1, bf16[256,128]{1,0:T(8,128)(2,1)} %refs_3_.1, bf16[256,128]{1,0:T(8,128)(2,1)} %refs_4_.1, bf16[1024,2048]{1,0:T(8,128)(2,1)} %refs_5_.1, ...), custom_call_target="tpu_custom_call" | custom-call | tf_op jit(solution)/shard_map/pallas_call | solution.py:1252
  87.5 0.7 copy.18
